TPU v7x, 32 devices: a whole 2x2x4 slice. The times are simulated.
32 devices in a mesh: fs: 16 (over z, y, x), tp: 2 (over core).
Axes of the slice: x: 2, y: 2, z: 4, core: 2. Of those that a mesh axis runs over, the one named last changes fastest.
Arguments:
- tokens: bfloat16 [3072, 2048], P('fs'), may hold values from -6 to 6
- route_ids: int32 [3072, 2], P('fs'), may hold values from 0 to 7, all different within a row; in each aligned block of 192 rows (0 to 191, 192 to 383, ...) at most 96 rows name the same one
- route_logits: float32 [3072, 2], P('fs'), may hold values from -6 to 6
- norm_gain: float32 [2048], P('fs'), may hold values from 0.1 to 1.9
- gate_weight: float32 [8, 2048, 2048], P(None, 'fs', 'tp'), may hold values from -0.125 to 0.125
- up_weight: float32 [8, 2048, 2048], P(None, 'fs', 'tp'), may hold values from -0.125 to 0.125
- down_weight: float32 [8, 2048, 2048], P(None, 'fs', 'tp'), may hold values from -0.125 to 0.125
Outputs:
- mixed: bfloat16 [3072, 2048], P('fs')
- gate_copies: bfloat16 [16, 2048, 2048], P('fs', None, 'tp')
- up_copies: bfloat16 [16, 2048, 2048], P('fs', None, 'tp')
- down_copies: bfloat16 [16, 2048, 2048], P('fs', None, 'tp')
Inputs may be any that keep to these rules, and one draw needn't show every extreme that they name: `route_ids`: each row names 2 different experts. Among the rows of one index of fs no expert is named by more than 96 rows, a bound that some of them reach.
All inputs are finite; a program needn't handle non-finite values.
Results may differ from a plain program's by a relative error of at most 0.014.
Values may be sent and summed in bfloat16 or wider, within the bound.
A program may use at most 128 MiB of HBM per device.

v0:
```python
import functools

import jax
import jax.numpy as jnp
from jax import lax
from jax.experimental import pallas as pl
from jax.experimental.pallas import tpu as pltpu
from jax.sharding import PartitionSpec as P

CAP = 96
STRIDE = 1
MESH = pl.DeviceIdType.MESH
BF16 = jnp.bfloat16
F32 = jnp.float32


def handoff(
    experts,
    copies,
    tps,
    tok,
    gain,
    gate_in,
    up_in,
    down_in,
    gate_out,
    up_out,
    down_out,
    back_out,
    stage,
    send,
    full,
    rows_in,
    hidden,
    part,
    part_in,
    share,
    back,
    load_sem,
    w_send,
    w_recv,
    r_send,
    r_recv,
    t_send,
    t_recv,
    tx_send,
    tx_recv,
    p_send,
    p_recv,
    b_send,
    b_recv,
    bx_send,
    bx_recv,
    out_sem,
    tok_sem,
):
    shard, cols = stage.shape[2], stage.shape[3]
    width = rows_in.shape[1]
    block = tok.shape[1]
    chunk_f = min(256, cols)
    chunk_w = width // experts
    n_f, n_w = cols // chunk_f, experts // tps
    me = lax.axis_index("fs")
    tp = lax.axis_index("tp")
    group = lax.div(me, copies)
    lane = lax.rem(me, copies)
    weights = (gate_in, up_in, down_in)
    outs = (gate_out, up_out, down_out)

    paired = experts & (experts - 1) == 0

    def ahead(d):
        if paired:
            return lax.bitwise_xor(group, lax.rem(jnp.int32(d) * STRIDE, experts))
        return lax.rem(group + d, experts)

    def behind(d):
        if paired:
            return ahead(d)
        return lax.rem(group + experts - d, experts)

    def twin(c):
        return lax.rem(lane + c, copies)

    def mate(p):
        return lax.rem(tp + p, tps)

    def slots(e):
        return pl.ds(pl.multiple_of(e * CAP, 32), CAP)

    def own_cols(q, j=0, size=block):
        return pl.ds(pl.multiple_of(q * block + j * chunk_w, 128), size)

    def shard_rows(g, c):
        return pl.ds(pl.multiple_of((g * copies + c) * shard, 32), shard)

    def loop(lo, hi, body):
        def step(i, carry):
            body(i)
            return carry

        lax.fori_loop(lo, hi, step, 0)

    def remote(src, dst, s_sem, r_sem, fs_to, tp_to):
        return pltpu.make_async_remote_copy(
            src_ref=src,
            dst_ref=dst,
            send_sem=s_sem,
            recv_sem=r_sem,
            device_id=(fs_to, tp_to),
            device_id_type=MESH,
        )

    def load(m, h):
        return pltpu.make_async_copy(weights[m].at[h], stage.at[m, h], load_sem.at[m, h])

    def direct(m, h, s):
        return remote(
            send.at[m, h],
            full.at[m, shard_rows(s, lane)],
            w_send.at[m, h],
            w_recv.at[m, s],
            h * copies + lane,
            tp,
        )

    def relay(m, s, c, to):
        return remote(
            full.at[m, shard_rows(s, c)],
            full.at[m, shard_rows(s, c)],
            r_send.at[m, s, to],
            r_recv.at[m, s, c],
            group * copies + to,
            tp,
        )

    def dispatch(h, s):
        return remote(
            tok.at[slots(h)],
            rows_in.at[slots(s), own_cols(tp)],
            t_send.at[h],
            t_recv.at[s],
            h * copies + lane,
            tp,
        )

    def spread(s, q, p):
        return remote(
            rows_in.at[slots(s), own_cols(q)],
            rows_in.at[slots(s), own_cols(q)],
            tx_send.at[s, p],
            tx_recv.at[s, p],
            me,
            mate(p),
        )

    def features(e):
        return pl.ds(pl.multiple_of(e * chunk_w, 128), chunk_w)

    def partial(e, q):
        owner, j = lax.div(e, n_w), lax.rem(e, n_w)
        p = lax.rem(owner - q + tps, tps)
        return remote(
            part.at[:, features(e)],
            part_in.at[p - 1, :, features(j)],
            p_send.at[e],
            p_recv.at[p, j],
            me,
            owner,
        )

    def give(s, e, j):
        where = pl.ds(pl.multiple_of(j * chunk_w, 128), chunk_w)
        return remote(
            share.at[slots(s), where],
            back.at[slots(e), own_cols(tp, j, chunk_w)],
            b_send.at[s, j],
            b_recv.at[e, j],
            s * copies + lane,
            tp,
        )

    def fan(e, q, j, p):
        return remote(
            back.at[slots(e), own_cols(q, j, chunk_w)],
            back.at[slots(e), own_cols(q, j, chunk_w)],
            bx_send.at[e, j, p],
            bx_recv.at[e, j, p],
            me,
            mate(p),
        )

    for m in range(3):
        loop(0, experts, lambda d, m=m: load(m, ahead(d)).start())
    tok_copy = pltpu.make_async_copy(
        tok.at[slots(group)], rows_in.at[slots(group), own_cols(tp)], tok_sem
    )
    tok_copy.start()

    barrier = pltpu.get_barrier_semaphore()
    for d in range(1, experts):
        pl.semaphore_signal(
            barrier, inc=1, device_id=(ahead(d) * copies + lane, tp), device_id_type=MESH
        )
    for c in range(1, copies):
        pl.semaphore_signal(
            barrier, inc=1, device_id=(group * copies + twin(c), tp), device_id_type=MESH
        )
    for p in range(1, tps):
        pl.semaphore_signal(barrier, inc=1, device_id=(me, mate(p)), device_id_type=MESH)
    pl.semaphore_wait(barrier, experts + copies + tps - 3)

    loop(1, experts, lambda d: dispatch(ahead(d), group).start())

    def rounded(m, h):
        load(m, h).wait()
        value = stage[m, h]
        if m < 2:
            value = gain[...] * value
        return value.astype(BF16)

    for m in range(3):
        full[m, shard_rows(group, lane)] = rounded(m, group)
    for m in range(3):
        def convert(d, m=m):
            send[m, ahead(d)] = rounded(m, ahead(d))

            @pl.when(d > 1)
            def _():
                direct(m, ahead(d - 1), group).start()

        loop(1, experts, convert)
        for c in range(1, copies):
            relay(m, group, lane, twin(c)).start()
        direct(m, ahead(experts - 1), group).start()

    tok_copy.wait()
    for p in range(1, tps):
        spread(group, tp, p).start()

    def spread_step(d):
        s = behind(d)
        dispatch(s, s).wait_recv()
        for p in range(1, tps):
            spread(s, tp, p).start()

    def relay_step(m, d):
        s = behind(d)
        direct(m, s, s).wait_recv()
        for c in range(1, copies):
            relay(m, s, lane, twin(c)).start()

    def relay_wait(m, s):
        for c in range(1, copies):
            relay(m, s, twin(c), lane).wait_recv()

    def out_copy(m):
        return pltpu.make_async_copy(full.at[m], outs[m].at[0], out_sem.at[m])

    loop(1, experts, spread_step)
    loop(1, experts, lambda d: relay_step(0, d))
    loop(1, experts, lambda d: relay_step(1, d))
    def spread_wait(s):
        for p in range(1, tps):
            spread(s, mate(tps - p), p).wait_recv()

    loop(0, experts, spread_wait)
    for m in range(2):
        loop(0, experts, lambda s, m=m: relay_wait(m, s))
        out_copy(m).start()

    def gate_up(c):
        @pl.when(c < experts - 1)
        def _():
            relay_step(2, 1 + c)

        where = pl.ds(pl.multiple_of(c * chunk_f, 128), chunk_f)
        gate = jnp.dot(rows_in[...], full[0, :, where], preferred_element_type=F32)
        up = jnp.dot(rows_in[...], full[1, :, where], preferred_element_type=F32)
        hidden[:, where] = (gate / (1.0 + jnp.exp(-gate)) * up).astype(BF16)

    loop(0, n_f, gate_up)
    def add_up(e):
        @pl.when(lax.div(e, n_w) == tp)
        def _():
            j = lax.rem(e, n_w)
            total = part[:, features(e)].astype(F32)
            for p in range(1, tps):
                partial(e, mate(tps - p)).wait_recv()
                total = total + part_in[p - 1, :, features(j)].astype(F32)
            share[:, features(j)] = total.astype(BF16)
            back[slots(group), features(e)] = share[slots(group), features(j)]
            loop(1, experts, lambda d: give(behind(d), group, j).start())
            for p in range(1, tps):
                fan(group, tp, j, p).start()

    def down_step(d):
        e = behind(d)

        @pl.when(d + n_f < experts - 1)
        def _():
            relay_step(2, d + n_f + 1)

        relay_wait(2, e)
        part[:, features(e)] = lax.dot_general(
            hidden[...],
            full[2, features(e), :],
            (((1,), (1,)), ((), ())),
            preferred_element_type=F32,
        ).astype(BF16)

        @pl.when(lax.div(e, n_w) != tp)
        def _():
            partial(e, tp).start()

        @pl.when(d > 0)
        def _():
            add_up(behind(d - 1))

    loop(0, experts, down_step)
    out_copy(2).start()
    add_up(behind(experts - 1))

    def back_step(j):
        def one(d):
            e = ahead(d)
            give(e, e, j).wait_recv()
            for p in range(1, tps):
                fan(e, tp, j, p).start()

        loop(1, experts, one)

    loop(0, n_w, back_step)

    def back_wait(j):
        def one(e):
            for p in range(1, tps):
                fan(e, mate(tps - p), j, p).wait_recv()

        loop(0, experts, one)

    loop(0, n_w, back_wait)
    last = pltpu.make_async_copy(back, back_out, tok_sem)
    last.start()

    loop(1, experts, lambda d: dispatch(ahead(d), group).wait_send())
    for m in range(3):
        loop(1, experts, lambda d, m=m: direct(m, ahead(d), group).wait_send())

        def relays(s, m=m):
            for c in range(1, copies):
                relay(m, s, lane, twin(c)).wait_send()

        loop(0, experts, relays)
        out_copy(m).wait()

    def spreads(s):
        for p in range(1, tps):
            spread(s, tp, p).wait_send()

    loop(0, experts, spreads)

    def part_sent(e):
        @pl.when(lax.div(e, n_w) != tp)
        def _():
            partial(e, tp).wait_send()

    loop(0, experts, part_sent)

    def tail(j):
        loop(1, experts, lambda d: give(behind(d), group, j).wait_send())

        def fans(e):
            for p in range(1, tps):
                fan(e, tp, j, p).wait_send()

        loop(0, experts, fans)

    loop(0, n_w, tail)
    last.wait()


def body(tokens, route_ids, route_logits, norm_gain, gate_weight, up_weight, down_weight):
    experts, shard, cols = gate_weight.shape
    fs_count, tps = lax.axis_size("fs"), lax.axis_size("tp")
    copies = fs_count // experts
    tok_rows, width = tokens.shape
    block = width // tps
    n_slots = experts * CAP
    depth = shard * fs_count

    values = tokens.astype(F32)
    center = jnp.mean(values, axis=1, keepdims=True)
    spread = jnp.mean(jnp.square(values - center), axis=1, keepdims=True)
    normed = ((values - center) * lax.rsqrt(spread + 1e-06)).astype(BF16)

    expert_ids = jnp.arange(experts, dtype=jnp.int32)[None, :]
    hit = [route_ids[:, k : k + 1] == expert_ids for k in range(2)]
    named = (hit[0] | hit[1]).astype(BF16)
    order = jnp.arange(tok_rows, dtype=jnp.int32)
    lower = (order[None, :] < order[:, None]).astype(BF16)
    rank = jnp.dot(lower, named, preferred_element_type=F32).astype(jnp.int32)
    place = expert_ids * CAP + rank
    slot = [jnp.sum(jnp.where(hit[k], place, 0), axis=1) for k in range(2)]
    slot_ids = jnp.arange(n_slots, dtype=jnp.int32)
    scatter = (
        (slot_ids[:, None] == slot[0][None, :]) | (slot_ids[:, None] == slot[1][None, :])
    ).astype(BF16)
    mine = lax.dynamic_slice_in_dim(normed, lax.axis_index("tp") * block, block, 1)
    tok = jnp.dot(scatter, mine, preferred_element_type=F32).astype(BF16)

    n_w = experts // tps
    dma = pltpu.SemaphoreType.DMA
    anywhere = pl.BlockSpec(memory_space=pl.ANY)
    copy_shape = jax.ShapeDtypeStruct((1, depth, cols), BF16)
    gate_new, up_new, down_new, returned = pl.pallas_call(
        functools.partial(handoff, experts, copies, tps),
        out_shape=(
            copy_shape,
            copy_shape,
            copy_shape,
            jax.ShapeDtypeStruct((n_slots, width), BF16),
        ),
        in_specs=[anywhere, pl.BlockSpec(memory_space=pltpu.VMEM)] + [anywhere] * 3,
        out_specs=(anywhere,) * 4,
        scratch_shapes=[
            pltpu.VMEM((3, experts, shard, cols), F32),
            pltpu.VMEM((3, experts, shard, cols), BF16),
            pltpu.VMEM((3, depth, cols), BF16),
            pltpu.VMEM((n_slots, width), BF16),
            pltpu.VMEM((n_slots, cols), BF16),
            pltpu.VMEM((n_slots, width), BF16),
            pltpu.VMEM((tps - 1, n_slots, block), BF16),
            pltpu.VMEM((n_slots, block), BF16),
            pltpu.VMEM((n_slots, width), BF16),
            dma((3, experts)),
            dma((3, experts)),
            dma((3, experts)),
            dma((3, experts, copies)),
            dma((3, experts, copies)),
            dma((experts,)),
            dma((experts,)),
            dma((experts, tps)),
            dma((experts, tps)),
            dma((experts,)),
            dma((tps, n_w)),
            dma((experts, n_w)),
            dma((experts, n_w)),
            dma((experts, n_w, tps)),
            dma((experts, n_w, tps)),
            dma((3,)),
            dma,
        ],
        compiler_params=pltpu.CompilerParams(
            collective_id=0, has_side_effects=True, vmem_limit_bytes=64 * 1024 * 1024 - 65536
        ),
        name="handoff",
    )(tok, norm_gain[:, None], gate_weight, up_weight, down_weight)

    picked = [
        jnp.dot(
            (slot[k][:, None] == slot_ids[None, :]).astype(BF16),
            returned,
            preferred_element_type=F32,
        )
        for k in range(2)
    ]
    first_weight = jax.nn.sigmoid(route_logits[:, 0] - route_logits[:, 1])
    second_weight = jax.nn.sigmoid(route_logits[:, 1] - route_logits[:, 0])
    mixed = (first_weight[:, None] * picked[0] + second_weight[:, None] * picked[1]).astype(BF16)
    return (mixed, gate_new, up_new, down_new)


def solution(mesh):
    return jax.shard_map(
        body,
        mesh=mesh,
        in_specs=(
            P("fs", None),
            P("fs", None),
            P("fs", None),
            P("fs"),
            P(None, "fs", "tp"),
            P(None, "fs", "tp"),
            P(None, "fs", "tp"),
        ),
        out_specs=(P("fs", None), P("fs", None, "tp"), P("fs", None, "tp"), P("fs", None, "tp")),
        check_vma=False,
    )
```

profile of v0, /device:TPU:1, one launch (start us, length us, event | category | flops | bytes accessed | tf_op | source)
XLA Modules:
  0.0 244.8 jit_solution(7990059401107350101)
XLA Ops:
  0.6 0.8 fusion.17
  1.4 0.2 select_reduce_fusion.1
  1.6 0.0 copy-start.4
  1.6 0.0 copy-start.6
  1.6 1.3 convert_reduce_fusion
  2.9 1.5 multiply_reduce_fusion
  4.4 0.0 copy-done.4
  4.5 0.0 copy-done.6
  4.5 1.8 convolution_convert_fusion.tok
  6.3 0.7 copy.11.gain
  7.0 222.2 %handoff.1 = (bf16[1,2048,1024]{2,1,0:T(8,128)(2,1)}, bf16[1,2048,1024]{2,1,0:T(8,128)(2,1)}, bf16[1,2048,1024]{2,1,0:T(8,128)(2,1)}, bf16[768,2048]{1,0:T(8,128)(2,1)}) custom-call(bf16[768,1024]{1,0:T(8,128)(2,1)} %convolution_convert_fusion.tok, f32[128,1]{1,0:T(8,128)} %copy.11.gain, f32[8,128,1024]{2,1,0:T(8,128)} %gate_in.1, f32[8,128,1024]{2,1,0:T(8,128)} %up_in.1, ...), custom_call_target="tpu_custom_call" | custom-call | tf_op jit(solution)/shard_map/handoff/pallas_call | solution.py:416
  229.3 0.8 add_divide_fusion
  230.0 0.0 copy-start.5
  230.0 2.9 %convolution_multiply_fusion.1 = f32[192,2048]{1,0:T(8,128)S(1)} fusion(bf16[768,2048]{1,0:T(8,128)(2,1)} %get-tuple-element.8, f32[192]{0:T(256)S(1)} %bitcast.8, s32[192]{0:T(256)} %copy-done.6), kind=kOutput, calls=%fused_computation.2 | convolution fusion | flops 604520448 | bytes 4720128 | tf_op jit(solution)/shard_map/dot_general | solution.py:461
  232.9 0.0 copy-done
  232.9 0.0 copy-done.5
  233.0 0.0 copy-start.3
  233.0 1.7 fusion.1
  234.7 0.7 copy-done.3
  235.4 2.1 copy.15
  237.6 1.6 copy-done.2
  239.1 2.1 copy.16
  241.3 1.6 copy-done.1
  242.8 2.0 copy.17
  (8 shorter events, 0.0 us)
Async XLA Ops:
  1.6 2.9 %copy-start.4 = (s32[192]{0:T(256)}, s32[192]{0:T(256)S(1)}, u32[]{:S(2)}) copy-start(s32[192]{0:T(256)S(1)} %get-tuple-element.13) | copy-start | bytes 2308
  1.6 2.9 %copy-start.6 = (s32[192]{0:T(256)}, s32[192]{0:T(256)S(1)}, u32[]{:S(2)}) copy-start(s32[192]{0:T(256)S(1)} %get-tuple-element.12) | copy-start | bytes 2308
  4.4 1.8 copy-start.7
  230.0 2.9 %copy-start = (bf16[768,2048]{1,0:T(8,128)(2,1)S(1)}, bf16[768,2048]{1,0:T(8,128)(2,1)}, u32[]{:S(2)}) copy-start(bf16[768,2048]{1,0:T(8,128)(2,1)} %get-tuple-element.8) | copy-start | bytes 9437188
  230.0 2.9 %copy-start.5 = (s32[192]{0:T(256)S(1)}, s32[192]{0:T(256)}, u32[]{:S(2)}) copy-start(s32[192]{0:T(256)} %copy-done.4) | copy-start | bytes 2308
  233.0 2.5 %copy-start.3 = (bf16[1,2048,1024]{2,1,0:T(8,128)(2,1)S(1)}, bf16[1,2048,1024]{2,1,0:T(8,128)(2,1)}, u32[]{:S(2)}) copy-start(bf16[1,2048,1024]{2,1,0:T(8,128)(2,1)} %get-tuple-element.25) | copy-start | bytes 12582916
  235.4 3.7 %copy-start.2 = (bf16[1,2048,1024]{2,1,0:T(8,128)(2,1)S(1)}, bf16[1,2048,1024]{2,1,0:T(8,128)(2,1)}, u32[]{:S(2)}) copy-start(bf16[1,2048,1024]{2,1,0:T(8,128)(2,1)} %get-tuple-element.26) | copy-start | bytes 12582916
  239.1 3.7 %copy-start.1 = (bf16[1,2048,1024]{2,1,0:T(8,128)(2,1)S(1)}, bf16[1,2048,1024]{2,1,0:T(8,128)(2,1)}, u32[]{:S(2)}) copy-start(bf16[1,2048,1024]{2,1,0:T(8,128)(2,1)} %get-tuple-element.27) | copy-start | bytes 12582916
where the time goes:
time: 245 us
  Pallas kernels  222 us (91%)
  local copies, waits for them, and re-layouts  11.7 us (5%)
  matrix products  6.59 us (3%)
  other arithmetic  3.59 us (1%)
    pallas_call x1, Pallas kernels, body(): pl.pallas_call(functools.partial(handoff, experts, copies, tps), out_shap...  222 us
    unnamed x19, local copies, waits for them, and re-layouts  10.2 us

commit v1 on v0

v1 whole, which is shorter than its diff:
```python
import functools
import math

import jax
import jax.numpy as jnp
from jax import lax
from jax.experimental import pallas as pl
from jax.experimental.pallas import tpu as pltpu
from jax.sharding import PartitionSpec as P

MESH = pl.DeviceIdType.MESH
BF16 = jnp.bfloat16
F32 = jnp.float32


def layer(
    experts,
    copies,
    tps,
    tokens,
    ids,
    logits,
    gain,
    gate_in,
    up_in,
    down_in,
    mixed_out,
    gate_out,
    up_out,
    down_out,
    tok,
    gain_col,
    stage,
    send,
    full,
    rows_in,
    table,
    scale,
    hidden,
    part,
    part_in,
    share,
    arrived,
    mixed,
    load_sem,
    w_send,
    w_recv,
    r_send,
    r_recv,
    t_send,
    t_recv,
    s_send,
    s_recv,
    tx_send,
    tx_recv,
    p_send,
    p_recv,
    g_send,
    g_recv,
    f_send,
    f_recv,
    out_sem,
    tok_sem,
):
    shard, cols = stage.shape[2], stage.shape[3]
    tok_rows, width = tok.shape
    block = width // tps
    chunk_f = min(256, cols)
    chunk_w = width // experts
    n_f, n_w = cols // chunk_f, experts // tps
    bits = experts.bit_length() - 1
    half = experts // 2
    me = lax.axis_index("fs")
    tp = lax.axis_index("tp")
    group = lax.div(me, copies)
    lane = lax.rem(me, copies)
    weights = (gate_in, up_in, down_in)
    outs = (gate_out, up_out, down_out)

    place = sum(
        lax.rem(lax.div(group, 1 << i), 2) * (1 << (bits - 1 - i)) for i in range(bits)
    )

    def ahead(d):
        return lax.bitwise_xor(group, jnp.int32(d))

    def twin(c):
        return lax.rem(lane + c, copies)

    def mate(p):
        return lax.rem(tp + p, tps)

    def kept(k):
        return lax.div(place, 1 << k) * (1 << k)

    def other(k):
        return lax.bitwise_xor(kept(k), jnp.int32(1 << k))

    def hop(k):
        return ahead(experts >> (k + 1)) * copies + lane

    def rows(b, k=0):
        return pl.ds(pl.multiple_of(b * tok_rows, 16), tok_rows << k)

    def own_cols(q):
        return pl.ds(pl.multiple_of(q * block, 128), block)

    def features(e):
        return pl.ds(pl.multiple_of(e * chunk_w, 128), chunk_w)

    def shard_rows(g, c):
        return pl.ds(pl.multiple_of((g * copies + c) * shard, 32), shard)

    def loop(lo, hi, body):
        def step(i, carry):
            body(i)
            return carry

        lax.fori_loop(lo, hi, step, 0)

    def remote(src, dst, s_sem, r_sem, fs_to, tp_to):
        return pltpu.make_async_remote_copy(
            src_ref=src,
            dst_ref=dst,
            send_sem=s_sem,
            recv_sem=r_sem,
            device_id=(fs_to, tp_to),
            device_id_type=MESH,
        )

    def load(m, h):
        return pltpu.make_async_copy(weights[m].at[h], stage.at[m, h], load_sem.at[m, h])

    def direct(m, h, s):
        return remote(
            send.at[m, h],
            full.at[m, shard_rows(s, lane)],
            w_send.at[m, h],
            w_recv.at[m, s],
            h * copies + lane,
            tp,
        )

    def relay(m, s, c, to):
        return remote(
            full.at[m, shard_rows(s, c)],
            full.at[m, shard_rows(s, c)],
            r_send.at[m, s, to],
            r_recv.at[m, s, c],
            group * copies + to,
            tp,
        )

    def gather(k, b):
        span = rows_in.at[rows(b, k), own_cols(tp)]
        return remote(span, span, t_send.at[k], t_recv.at[k], hop(k), tp)

    def share_table(k, b):
        span = table.at[pl.ds(b, 1 << k)]
        return remote(span, span, s_send.at[k], s_recv.at[k], hop(k), tp)

    def spread(k, q, p):
        span = rows_in.at[rows(other(k), k), own_cols(q)]
        return remote(span, span, tx_send.at[k, p], tx_recv.at[k, p], me, mate(p))

    def partial(e):
        owner, j = lax.rem(e, tps), lax.div(e, tps)
        p = lax.rem(owner - tp + tps, tps)
        return remote(
            part.at[:, features(e)],
            part_in.at[p - 1, :, features(j)],
            p_send.at[e],
            p_recv.at[p - 1, j],
            me,
            owner,
        )

    def partial_in(p, j):
        span = part_in.at[p - 1, :, features(j)]
        return remote(span, span, p_send.at[0], p_recv.at[p - 1, j], me, mate(p))

    def landing(k):
        return pl.ds(((1 << k) - 1) * tok_rows, tok_rows << k)

    def reduce(k, j):
        return remote(
            share.at[rows(other(k), k), features(j)],
            arrived.at[landing(k), features(j)],
            g_send.at[k, j],
            g_recv.at[k, j],
            hop(k),
            tp,
        )

    def fan(q, j, p):
        span = mixed.at[:, features(j * tps + q)]
        return remote(span, span, f_send.at[j, p], f_recv.at[j, p], me, mate(p))

    tok_copy = pltpu.make_async_copy(tokens, tok, tok_sem)
    tok_copy.start()
    for m in range(3):
        loop(0, experts, lambda d, m=m: load(m, ahead(d)).start())

    barrier = pltpu.get_barrier_semaphore()
    for d in range(1, experts):
        pl.semaphore_signal(
            barrier, inc=1, device_id=(ahead(d) * copies + lane, tp), device_id_type=MESH
        )
    for c in range(1, copies):
        pl.semaphore_signal(
            barrier, inc=1, device_id=(group * copies + twin(c), tp), device_id_type=MESH
        )
    for p in range(1, tps):
        pl.semaphore_signal(barrier, inc=1, device_id=(me, mate(p)), device_id_type=MESH)

    down_rows = lax.broadcasted_iota(jnp.int32, (shard, shard), 0)
    across = lax.broadcasted_iota(jnp.int32, (shard, shard), 1)
    gain_col[...] = jnp.sum(
        jnp.where(down_rows == across, gain[...], 0.0), axis=1, keepdims=True
    )

    gap = logits[0:1, :] - logits[1:2, :]
    choice = (1.0 / (1.0 + jnp.exp(-gap)), 1.0 / (1.0 + jnp.exp(gap)))
    named = lax.broadcasted_iota(jnp.int32, (experts, tok_rows), 0)
    table[place] = jnp.zeros(table.shape[1:], F32)
    table[place, :, 0:tok_rows] = sum(
        jnp.where(ids[k : k + 1, :] == named, choice[k], 0.0) for k in range(2)
    )

    tok_copy.wait()
    step_rows = math.gcd(tok_rows, 32)

    def normalize(i):
        at = pl.multiple_of(i * step_rows, 16)
        values = tok[pl.ds(at, step_rows), :].astype(F32)
        values = values - jnp.mean(values, axis=1, keepdims=True)
        var = jnp.mean(values * values, axis=1, keepdims=True)
        where = pl.ds(pl.multiple_of(place * tok_rows + at, 16), step_rows)
        rows_in[where, :] = (values * lax.rsqrt(var + 1e-06)).astype(BF16)

    loop(0, tok_rows // step_rows, normalize)

    def rounded(m, h):
        load(m, h).wait()
        value = stage[m, h]
        if m < 2:
            value = gain_col[...] * value
        return value.astype(BF16)

    full[0, shard_rows(group, lane)] = rounded(0, group)

    pl.semaphore_wait(barrier, experts + copies + tps - 3)

    gather(0, kept(0)).start()
    share_table(0, kept(0)).start()

    def convert(m, lo, hi):
        def one(d):
            send[m, ahead(d)] = rounded(m, ahead(d))

        loop(lo, hi, one)

    def start(m, lo, hi):
        loop(lo, hi, lambda d: direct(m, ahead(d), group).start())

    def relay_own(m):
        for c in range(1, copies):
            relay(m, group, lane, twin(c)).start()

    early = half + max(half // 2, 1)
    convert(0, half, early)
    relay_own(0)
    start(0, half, early)
    convert(0, 1, 2)
    for m in range(1, 3):
        full[m, shard_rows(group, lane)] = rounded(m, group)
        start(m - 1, 1, 2)
        convert(m, 1, 2)
        relay_own(m)
    start(2, 1, 2)
    convert(0, early, experts)
    convert(0, 2, half)
    convert(1, half, experts)
    convert(1, 2, half)
    convert(2, half, experts)
    convert(2, 2, half)

    def relay_step(m, d):
        s = ahead(d)
        direct(m, s, s).wait_recv()
        for c in range(1, copies):
            relay(m, s, lane, twin(c)).start()

    def relay_wait(m, s):
        for c in range(1, copies):
            relay(m, s, twin(c), lane).wait_recv()

    def gathered(k):
        gather(k, other(k)).wait_recv()
        share_table(k, other(k)).wait_recv()
        if k + 1 < bits:
            gather(k + 1, kept(k + 1)).start()
            share_table(k + 1, kept(k + 1)).start()
        for p in range(1, tps):
            spread(k, tp, p).start()

    def relays(m, lo, hi):
        loop(lo, hi, lambda d: relay_step(m, d))

    for m in range(3):
        relays(m, 1, 2)
    gathered(0)
    start(0, early, experts)
    start(0, 2, half)
    start(1, half, early)
    relays(0, half, early)
    for k in range(1, bits - 1):
        gathered(k)
    start(1, early, experts)
    start(1, 2, half)
    relays(0, 2, half)
    relays(0, early, experts)
    start(2, half, experts)
    start(2, 2, half)
    relays(1, half, early)
    relays(1, 2, half)
    gathered(bits - 1)
    relays(1, early, experts)

    def set_scale(b):
        row = table[b, pl.ds(group, 1), :]
        column = jnp.transpose(jnp.broadcast_to(row, (128, row.shape[1])))
        scale[rows(b), :] = column[:tok_rows]

    loop(0, experts, set_scale)

    def out_copy(m):
        return pltpu.make_async_copy(full.at[m], outs[m].at[0], out_sem.at[m])

    for m in range(2):
        loop(0, experts, lambda s, m=m: relay_wait(m, s))
        out_copy(m).start()

    n_pre = min(half - 1, 2 * n_f)
    for part_no in range(2):
        last = bits - 1
        span = rows((kept(last), other(last))[part_no], last)
        for k in range(bits - 1) if part_no == 0 else (bits - 1,):
            for p in range(1, tps):
                spread(k, mate(tps - p), p).wait_recv()

        def gate_up(c):
            if part_no == 0:
                @pl.when(c < min(n_pre, n_f))
                def _():
                    relay_step(2, 2 + c)

            where = pl.ds(pl.multiple_of(c * chunk_f, 128), chunk_f)
            gate = jnp.dot(rows_in[span, :], full[0, :, where], preferred_element_type=F32)
            up = jnp.dot(rows_in[span, :], full[1, :, where], preferred_element_type=F32)
            hidden[span, where] = (gate / (1.0 + jnp.exp(-gate)) * up).astype(BF16)

        loop(0, n_f, gate_up)

    relays(2, 2 + min(n_pre, n_f), half + 1)

    def add_up(e):
        @pl.when(lax.rem(e, tps) == tp)
        def _():
            j = lax.div(e, tps)
            for p in range(1, tps):
                partial_in(p, j).wait_recv()

            def one(b):
                for q in range(chunk_w // 128):
                    here = pl.ds(pl.multiple_of(e * chunk_w + q * 128, 128), 128)
                    there = pl.ds(pl.multiple_of(j * chunk_w + q * 128, 128), 128)
                    total = part[rows(b), here].astype(F32)
                    for p in range(1, tps):
                        total = total + part_in[p - 1, rows(b), there].astype(F32)
                    share[rows(b), there] = (scale[rows(b), :] * total).astype(BF16)

            first = other(bits - 1)
            loop(first, first + half, one)
            reduce(bits - 1, j).start()
            first = kept(bits - 1)
            loop(first, first + half, one)

    def down_step(d):
        e = ahead(d)
        relay_wait(2, e)
        part[:, features(e)] = lax.dot_general(
            hidden[...],
            full[2, features(e), :],
            (((1,), (1,)), ((), ())),
            preferred_element_type=F32,
        ).astype(BF16)

        @pl.when(lax.rem(e, tps) != tp)
        def _():
            partial(e).start()

    def owned(i):
        e = ahead(tps * i + lax.bitwise_xor(tp, lax.rem(group, tps)))
        return lax.div(e, tps)

    def reduce_step(k, i):
        j = owned(i)
        reduce(k, j).wait_recv()

        def one(b):
            here = rows(kept(k) + b)
            come = pl.ds(pl.multiple_of(((1 << k) - 1 + b) * tok_rows, 16), tok_rows)
            total = share[here, features(j)].astype(F32) + arrived[come, features(j)].astype(F32)
            if k > 0:
                share[here, features(j)] = total.astype(BF16)
            else:
                mixed[:, features(j * tps + tp)] = total.astype(BF16)

        loop(0, 1 << k, one)
        if k > 0:
            reduce(k - 1, j).start()
        else:
            for p in range(1, tps):
                fan(tp, j, p).start()

    def near_step(d):
        down_step(d)

        @pl.when(d > 0)
        def _():
            add_up(ahead(d - 1))

    loop(0, half, near_step)
    relays(2, half + 1, early)
    add_up(ahead(half - 1))
    for k in range(bits - 1, 0, -1):
        loop(0, n_w // 2, lambda i, k=k: reduce_step(k, i))

    def far_step(d):
        down_step(d)

        @pl.when(d > half)
        def _():
            add_up(ahead(d - 1))

        @pl.when(d + early - half < experts)
        def _():
            relay_step(2, d + early - half)

    loop(half, experts, far_step)
    out_copy(2).start()
    add_up(ahead(experts - 1))
    for k in range(bits - 1, 0, -1):
        loop(n_w // 2, n_w, lambda i, k=k: reduce_step(k, i))
    loop(n_w // 2, n_w, lambda i: reduce_step(0, i))
    loop(0, n_w // 2, lambda i: reduce_step(0, i))

    def fan_wait(j):
        for p in range(1, tps):
            fan(mate(tps - p), j, p).wait_recv()

    loop(0, n_w, fan_wait)
    last_copy = pltpu.make_async_copy(mixed, mixed_out, tok_sem)
    last_copy.start()

    for k in range(bits):
        gather(k, kept(k)).wait_send()
        share_table(k, kept(k)).wait_send()
        for p in range(1, tps):
            spread(k, tp, p).wait_send()
        loop(0, n_w, lambda j, k=k: reduce(k, j).wait_send())
    for m in range(3):
        loop(1, experts, lambda d, m=m: direct(m, ahead(d), group).wait_send())

        def relays_sent(s, m=m):
            for c in range(1, copies):
                relay(m, s, lane, twin(c)).wait_send()

        loop(0, experts, relays_sent)
        out_copy(m).wait()

    def part_sent(e):
        @pl.when(lax.rem(e, tps) != tp)
        def _():
            partial(e).wait_send()

    loop(0, experts, part_sent)

    def fans_sent(j):
        for p in range(1, tps):
            fan(tp, j, p).wait_send()

    loop(0, n_w, fans_sent)
    last_copy.wait()


def body(tokens, route_ids, route_logits, norm_gain, gate_weight, up_weight, down_weight):
    experts, shard, cols = gate_weight.shape
    fs_count, tps = lax.axis_size("fs"), lax.axis_size("tp")
    copies = fs_count // experts
    tok_rows, width = tokens.shape
    block = width // tps
    n_rows = experts * tok_rows
    depth = shard * fs_count
    n_w = experts // tps
    bits = experts.bit_length() - 1
    assert experts == 1 << bits and bits > 1
    assert tps & (tps - 1) == 0 and n_w * tps == experts

    dma = pltpu.SemaphoreType.DMA
    anywhere = pl.BlockSpec(memory_space=pl.ANY)
    inside = pl.BlockSpec(memory_space=pltpu.VMEM)
    copy_shape = jax.ShapeDtypeStruct((1, depth, cols), BF16)
    return pl.pallas_call(
        functools.partial(layer, experts, copies, tps),
        out_shape=(jax.ShapeDtypeStruct((tok_rows, width), BF16),) + (copy_shape,) * 3,
        in_specs=[anywhere] + [inside] * 3 + [anywhere] * 3,
        out_specs=(anywhere,) * 4,
        scratch_shapes=[
            pltpu.VMEM((tok_rows, width), BF16),
            pltpu.VMEM((shard, 1), F32),
            pltpu.VMEM((3, experts, shard, cols), F32),
            pltpu.VMEM((3, experts, shard, cols), BF16),
            pltpu.VMEM((3, depth, cols), BF16),
            pltpu.VMEM((n_rows, width), BF16),
            pltpu.VMEM((experts, experts, -(-tok_rows // 128) * 128), F32),
            pltpu.VMEM((n_rows, 128), F32),
            pltpu.VMEM((n_rows, cols), BF16),
            pltpu.VMEM((n_rows, width), BF16),
            pltpu.VMEM((tps - 1, n_rows, block), BF16),
            pltpu.VMEM((n_rows, block), BF16),
            pltpu.VMEM((n_rows - tok_rows, block), BF16),
            pltpu.VMEM((tok_rows, width), BF16),
            dma((3, experts)),
            dma((3, experts)),
            dma((3, experts)),
            dma((3, experts, copies)),
            dma((3, experts, copies)),
            dma((bits,)),
            dma((bits,)),
            dma((bits,)),
            dma((bits,)),
            dma((bits, tps)),
            dma((bits, tps)),
            dma((experts,)),
            dma((tps - 1, n_w)),
            dma((bits, n_w)),
            dma((bits, n_w)),
            dma((n_w, tps)),
            dma((n_w, tps)),
            dma((3,)),
            dma,
        ],
        compiler_params=pltpu.CompilerParams(
            collective_id=0, has_side_effects=True, vmem_limit_bytes=64 * 1024 * 1024 - 65536
        ),
        name="layer",
    )(
        tokens,
        route_ids.T,
        route_logits.T,
        norm_gain[None, :],
        gate_weight,
        up_weight,
        down_weight,
    )


def solution(mesh):
    return jax.shard_map(
        body,
        mesh=mesh,
        in_specs=(
            P("fs", None),
            P("fs", None),
            P("fs", None),
            P("fs"),
            P(None, "fs", "tp"),
            P(None, "fs", "tp"),
            P(None, "fs", "tp"),
        ),
        out_specs=(P("fs", None), P("fs", None, "tp"), P("fs", None, "tp"), P("fs", None, "tp")),
        check_vma=False,
    )
```

time: 245 us -> 267 us (1.090); the launches traced: 245 us -> 262 us
  Pallas kernels: 222 us -> 249 us
  matrix products: 6.59 us -> 0 us
  other arithmetic: 3.59 us -> 0 us
    pallas_call x1, Pallas kernels: 222 us -> 249 us  [body(): pl.pallas_call(functools.partial(layer, experts, copies, tps), out_shape=...]
    dot_general x4 -> x0, matrix products: 6.59 us -> none  [the longest x2 4.6 us: body(): jnp.dot((slot[k][:, None] == slot_ids[None, :]).astype(BF16), returned, p...]
    reduce_sum x2 -> x0, other arithmetic: 2.81 us -> none  [the longest x1 1.49 us: body(): spread = jnp.mean(jnp.square(values - center), axis=1, keepdims=True)]
    unnamed x19 -> x8, local copies, waits for them, and re-layouts: 10.2 us -> 12.6 us
where the time goes in v1:
time: 267 us; the launch traced here: 262 us
  Pallas kernels  249 us (93%)
  local copies, waits for them, and re-layouts  12.6 us (5%)
    pallas_call x1, Pallas kernels, body(): pl.pallas_call(functools.partial(layer, experts, copies, tps), out_shape=...  249 us
    unnamed x8, local copies, waits for them, and re-layouts  12.6 us

profile of v1, /device:TPU:1, one launch (start us, length us, event | category | flops | bytes accessed | tf_op | source)
XLA Modules:
  0.0 262.5 jit_solution(14001136934477483246)
XLA Ops:
  0.6 249.2 %layer.1 = (bf16[192,2048]{1,0:T(8,128)(2,1)}, bf16[1,2048,1024]{2,1,0:T(8,128)(2,1)}, bf16[1,2048,1024]{2,1,0:T(8,128)(2,1)}, bf16[1,2048,1024]{2,1,0:T(8,128)(2,1)}) custom-call(bf16[192,2048]{1,0:T(8,128)(2,1)} %tokens.1, s32[2,192]{1,0:T(2,128)} %bitcast.3, f32[2,192]{1,0:T(2,128)} %bitcast.4, f32[1,128]{1,0:T(1,128)} %bitcast.5, ...), custom_call_target="tpu_custom_call" | custom-call | tf_op jit(solution)/shard_map/layer/pallas_call | solution.py:515
  249.9 2.1 copy.15
  251.9 0.0 copy-start.1
  251.9 4.8 %copy.16 = bf16[1,2048,1024]{2,1,0:T(8,128)(2,1)} copy(bf16[1,2048,1024]{2,1,0:T(8,128)(2,1)} %get-tuple-element.9) | data formatting | bytes 8388608
  256.8 0.0 copy-done.1
  256.8 0.0 copy-start
  256.8 2.1 copy.17
  258.9 1.6 copy-done
  260.5 2.0 copy.18
Async XLA Ops:
  251.9 4.8 %copy-start.1 = (bf16[1,2048,1024]{2,1,0:T(8,128)(2,1)S(1)}, bf16[1,2048,1024]{2,1,0:T(8,128)(2,1)}, u32[]{:S(2)}) copy-start(bf16[1,2048,1024]{2,1,0:T(8,128)(2,1)} %get-tuple-element.10) | copy-start | bytes 12582916
  256.8 3.7 %copy-start = (bf16[1,2048,1024]{2,1,0:T(8,128)(2,1)S(1)}, bf16[1,2048,1024]{2,1,0:T(8,128)(2,1)}, u32[]{:S(2)}) copy-start(bf16[1,2048,1024]{2,1,0:T(8,128)(2,1)} %get-tuple-element.11) | copy-start | bytes 12582916

commit v2 on v1

--- a/solution.py
+++ b/solution.py
@@ -8,6 +8,7 @@
 from jax.experimental.pallas import tpu as pltpu
 from jax.sharding import PartitionSpec as P
 
+CAP = 96
 MESH = pl.DeviceIdType.MESH
 BF16 = jnp.bfloat16
 F32 = jnp.float32
@@ -35,10 +36,15 @@
     full,
     rows_in,
     table,
+    rank,
+    packed,
+    unpack,
     scale,
     hidden,
     part,
     part_in,
+    outbox,
+    pair,
     share,
     arrived,
     mixed,
@@ -77,10 +83,19 @@
     weights = (gate_in, up_in, down_in)
     outs = (gate_out, up_out, down_out)
 
+    def mirror(o):
+        return int(f"{o:0{bits}b}"[::-1], 2)
+
     place = sum(
         lax.rem(lax.div(group, 1 << i), 2) * (1 << (bits - 1 - i)) for i in range(bits)
     )
 
+    at_end = lax.rem(lax.div(group, half), 2) == lax.rem(lax.div(group, half // 2), 2)
+
+    def turn(d):
+        swapped = lax.bitwise_xor(jnp.int32(d), jnp.int32(half // 2))
+        return lax.select(jnp.logical_and(at_end, d >= half), swapped, jnp.int32(d))
+
     def ahead(d):
         return lax.bitwise_xor(group, jnp.int32(d))
 
@@ -101,6 +116,9 @@
 
     def rows(b, k=0):
         return pl.ds(pl.multiple_of(b * tok_rows, 16), tok_rows << k)
+
+    def slots(b):
+        return pl.ds(pl.multiple_of(b * CAP, 16), CAP)
 
     def own_cols(q):
         return pl.ds(pl.multiple_of(q * block, 128), block)
@@ -151,17 +169,26 @@
             tp,
         )
 
-    def gather(k, b):
-        span = rows_in.at[rows(b, k), own_cols(tp)]
-        return remote(span, span, t_send.at[k], t_recv.at[k], hop(k), tp)
-
-    def share_table(k, b):
-        span = table.at[pl.ds(b, 1 << k)]
-        return remote(span, span, s_send.at[k], s_recv.at[k], hop(k), tp)
-
-    def spread(k, q, p):
-        span = rows_in.at[rows(other(k), k), own_cols(q)]
-        return remote(span, span, tx_send.at[k, p], tx_recv.at[k, p], me, mate(p))
+    def at_offset(o):
+        return lax.bitwise_xor(place, jnp.int32(mirror(o)))
+
+    def gather(o, b):
+        span = rows_in.at[rows(at_offset(o)), own_cols(tp)]
+        return remote(span, span, t_send.at[o ^ b], t_recv.at[o ^ b], ahead(b) * copies + lane, tp)
+
+    def share_table(o, b):
+        span = table.at[at_offset(o)]
+        return remote(span, span, s_send.at[o ^ b], s_recv.at[o ^ b], ahead(b) * copies + lane, tp)
+
+    def gather_in(o):
+        span, row = rows_in.at[rows(at_offset(o)), own_cols(tp)], table.at[at_offset(o)]
+        b = ahead(o & -o) * copies + lane
+        remote(span, span, t_send.at[o], t_recv.at[o], b, tp).wait_recv()
+        remote(row, row, s_send.at[o], s_recv.at[o], b, tp).wait_recv()
+
+    def spread(o, q, p):
+        span = rows_in.at[rows(at_offset(o)), own_cols(q)]
+        return remote(span, span, tx_send.at[o, p], tx_recv.at[o, p], me, mate(p))
 
     def partial(e):
         owner, j = lax.rem(e, tps), lax.div(e, tps)
@@ -183,14 +210,13 @@
         return pl.ds(((1 << k) - 1) * tok_rows, tok_rows << k)
 
     def reduce(k, j):
-        return remote(
-            share.at[rows(other(k), k), features(j)],
-            arrived.at[landing(k), features(j)],
-            g_send.at[k, j],
-            g_recv.at[k, j],
-            hop(k),
-            tp,
-        )
+        if k == bits - 1:
+            src = outbox.at[:, :, features(j)]
+            dst = pair.at[:, pl.ds(CAP, CAP), features(j)]
+        else:
+            src = share.at[rows(other(k) - kept(bits - 1), k), features(j)]
+            dst = arrived.at[landing(k), features(j)]
+        return remote(src, dst, g_send.at[k, j], g_recv.at[k, j], hop(k), tp)
 
     def fan(q, j, p):
         span = mixed.at[:, features(j * tps + q)]
@@ -227,6 +253,7 @@
         jnp.where(ids[k : k + 1, :] == named, choice[k], 0.0) for k in range(2)
     )
 
+    phase = jax.named_scope
     tok_copy.wait()
     step_rows = math.gcd(tok_rows, 32)
 
@@ -249,10 +276,18 @@
 
     full[0, shard_rows(group, lane)] = rounded(0, group)
 
-    pl.semaphore_wait(barrier, experts + copies + tps - 3)
-
-    gather(0, kept(0)).start()
-    share_table(0, kept(0)).start()
+    with phase("barrier"):
+        pl.semaphore_wait(barrier, experts + copies + tps - 3)
+
+    masks = [1 << k for k in range(bits - 1, -1, -1)]
+
+    def forward(o):
+        for b in masks:
+            if o == 0 or b < o & -o:
+                gather(o, b).start()
+                share_table(o, b).start()
+
+    forward(0)
 
     def convert(m, lo, hi):
         def one(d):
@@ -267,26 +302,8 @@
         for c in range(1, copies):
             relay(m, group, lane, twin(c)).start()
 
-    early = half + max(half // 2, 1)
-    convert(0, half, early)
-    relay_own(0)
-    start(0, half, early)
-    convert(0, 1, 2)
-    for m in range(1, 3):
-        full[m, shard_rows(group, lane)] = rounded(m, group)
-        start(m - 1, 1, 2)
-        convert(m, 1, 2)
-        relay_own(m)
-    start(2, 1, 2)
-    convert(0, early, experts)
-    convert(0, 2, half)
-    convert(1, half, experts)
-    convert(1, 2, half)
-    convert(2, half, experts)
-    convert(2, 2, half)
-
     def relay_step(m, d):
-        s = ahead(d)
+        s = ahead(turn(d) if m < 2 else d)
         direct(m, s, s).wait_recv()
         for c in range(1, copies):
             relay(m, s, lane, twin(c)).start()
@@ -295,74 +312,140 @@
         for c in range(1, copies):
             relay(m, s, twin(c), lane).wait_recv()
 
-    def gathered(k):
-        gather(k, other(k)).wait_recv()
-        share_table(k, other(k)).wait_recv()
-        if k + 1 < bits:
-            gather(k + 1, kept(k + 1)).start()
-            share_table(k + 1, kept(k + 1)).start()
+    def gathered(o):
+        gather_in(o)
+        forward(o)
         for p in range(1, tps):
-            spread(k, tp, p).start()
+            spread(o, tp, p).start()
 
     def relays(m, lo, hi):
         loop(lo, hi, lambda d: relay_step(m, d))
 
-    for m in range(3):
-        relays(m, 1, 2)
-    gathered(0)
-    start(0, early, experts)
-    start(0, 2, half)
-    start(1, half, early)
-    relays(0, half, early)
-    for k in range(1, bits - 1):
-        gathered(k)
-    start(1, early, experts)
-    start(1, 2, half)
-    relays(0, 2, half)
-    relays(0, early, experts)
-    start(2, half, experts)
-    start(2, 2, half)
-    relays(1, half, early)
-    relays(1, 2, half)
-    gathered(bits - 1)
-    relays(1, early, experts)
-
-    def set_scale(b):
-        row = table[b, pl.ds(group, 1), :]
-        column = jnp.transpose(jnp.broadcast_to(row, (128, row.shape[1])))
-        scale[rows(b), :] = column[:tok_rows]
-
-    loop(0, experts, set_scale)
-
     def out_copy(m):
         return pltpu.make_async_copy(full.at[m], outs[m].at[0], out_sem.at[m])
 
-    for m in range(2):
-        loop(0, experts, lambda s, m=m: relay_wait(m, s))
-        out_copy(m).start()
-
-    n_pre = min(half - 1, 2 * n_f)
-    for part_no in range(2):
-        last = bits - 1
-        span = rows((kept(last), other(last))[part_no], last)
-        for k in range(bits - 1) if part_no == 0 else (bits - 1,):
+    early = half + max(half // 2, 1)
+    with phase("first"):
+        convert(0, 2, early)
+        relay_own(0)
+        start(0, 2, early)
+        convert(0, 1, 2)
+        for m in range(1, 3):
+            full[m, shard_rows(group, lane)] = rounded(m, group)
+            start(m - 1, 1, 2)
+            convert(m, 1, 2)
+            relay_own(m)
+        start(2, 1, 2)
+        convert(0, early, experts)
+        convert(1, 2, experts)
+        convert(2, 2, experts)
+    with phase("gate_1"):
+        relays(0, 1, 2)
+    for o in range(2, half, 2):
+        with phase("tok_low"):
+            gathered(o)
+    with phase("tok_half"):
+        gathered(half)
+    start(0, early, experts)
+    start(1, 2, experts)
+    with phase("up_down_1"):
+        relays(1, 1, 2)
+        relays(2, 1, 2)
+    with phase("gate_near"):
+        relays(0, 2, half)
+    for o in range(half + 2, experts, 2):
+        with phase("tok_high"):
+            gathered(o)
+    start(2, 2, half)
+    with phase("gate_far"):
+        relays(0, half, experts)
+    for o in range(1, experts, 2):
+        with phase("tok_odd"):
+            gathered(o)
+
+    with phase("gate_wait"):
+        for o in range(1, experts):
             for p in range(1, tps):
-                spread(k, mate(tps - p), p).wait_recv()
-
-        def gate_up(c):
-            if part_no == 0:
-                @pl.when(c < min(n_pre, n_f))
+                spread(o, mate(tps - p), p).wait_recv()
+
+    lanes = table.shape[2]
+    before = lax.broadcasted_iota(jnp.int32, (lanes, lanes), 0)
+    after = lax.broadcasted_iota(jnp.int32, (lanes, lanes), 1)
+    earlier = jnp.where(before < after, 1.0, 0.0).astype(BF16)
+
+    def set_rank(b):
+        chosen = table[b] > 0.0
+        count = jnp.dot(
+            jnp.where(chosen, 1.0, 0.0).astype(BF16), earlier, preferred_element_type=F32
+        )
+        rank[b] = jnp.where(chosen, count, -4.0 * CAP)
+
+    def pack(b):
+        slot = lax.broadcasted_iota(jnp.int32, (CAP, lanes), 0).astype(F32)
+        hit = jnp.where(rank[b, pl.ds(group, 1), :] == slot, 1.0, 0.0)
+        weight = jnp.sum(hit * table[b, pl.ds(group, 1), :], axis=1, keepdims=True)
+        scale[slots(b), :] = jnp.broadcast_to(weight, (CAP, 128))
+        packed[slots(b), :] = jnp.dot(
+            hit[:, :tok_rows].astype(BF16), rows_in[rows(b), :], preferred_element_type=F32
+        ).astype(BF16)
+
+    def column(b, e):
+        row = rank[b, pl.ds(e, 1), :]
+        return jnp.transpose(jnp.broadcast_to(row, (128, lanes)))[:tok_rows, 0:1]
+
+    def set_unpack(i):
+        b = kept(bits - 1) + i
+        slot = lax.broadcasted_iota(jnp.int32, (tok_rows, 2 * CAP), 1).astype(F32)
+        hit = (column(b, group) == slot) | (column(b, ahead(1)) + CAP == slot)
+        unpack[i] = jnp.where(hit, 1.0, 0.0).astype(BF16)
+
+    with phase("set_rank"):
+        loop(0, experts, set_rank)
+    with phase("pack"):
+        loop(0, experts, pack)
+    with phase("set_unpack"):
+        loop(0, half, set_unpack)
+
+    def project(m, pending):
+        def one(c):
+            for slot, d in pending:
+                @pl.when(c == min(slot, n_f - 1))
                 def _():
-                    relay_step(2, 2 + c)
+                    with phase("relay_in"):
+                        relay_step(m + 1, d)
 
             where = pl.ds(pl.multiple_of(c * chunk_f, 128), chunk_f)
-            gate = jnp.dot(rows_in[span, :], full[0, :, where], preferred_element_type=F32)
-            up = jnp.dot(rows_in[span, :], full[1, :, where], preferred_element_type=F32)
-            hidden[span, where] = (gate / (1.0 + jnp.exp(-gate)) * up).astype(BF16)
-
-        loop(0, n_f, gate_up)
-
-    relays(2, 2 + min(n_pre, n_f), half + 1)
+            out = jnp.dot(packed[...], full[m, :, where], preferred_element_type=F32)
+            if m == 0:
+                out = out / (1.0 + jnp.exp(-out))
+            else:
+                out = out * hidden[:, where].astype(F32)
+            hidden[:, where] = out.astype(BF16)
+
+        with phase("project"):
+            loop(0, n_f, one)
+
+    with phase("gate_wait"):
+        loop(0, experts, lambda s: relay_wait(0, s))
+        out_copy(0).start()
+    project(0, [(i, 2 + i) for i in range(half)])
+
+    @pl.when(jnp.logical_not(at_end))
+    def _():
+        start(2, half, experts)
+
+    with phase("up_rest"):
+        relays(1, 2 + half, experts)
+
+    with phase("up_wait"):
+        loop(0, experts, lambda s: relay_wait(1, s))
+        out_copy(1).start()
+
+    @pl.when(at_end)
+    def _():
+        start(2, half, experts)
+
+    project(1, [(2 * i, 2 + i) for i in range(half - 2)])
 
     def add_up(e):
         @pl.when(lax.rem(e, tps) == tp)
@@ -371,20 +454,22 @@
             for p in range(1, tps):
                 partial_in(p, j).wait_recv()
 
-            def one(b):
-                for q in range(chunk_w // 128):
-                    here = pl.ds(pl.multiple_of(e * chunk_w + q * 128, 128), 128)
-                    there = pl.ds(pl.multiple_of(j * chunk_w + q * 128, 128), 128)
-                    total = part[rows(b), here].astype(F32)
-                    for p in range(1, tps):
-                        total = total + part_in[p - 1, rows(b), there].astype(F32)
-                    share[rows(b), there] = (scale[rows(b), :] * total).astype(BF16)
-
-            first = other(bits - 1)
-            loop(first, first + half, one)
+            def fill(target, first):
+                def one(i):
+                    b = first + i
+                    for q in range(chunk_w // 128):
+                        here = pl.ds(pl.multiple_of(e * chunk_w + q * 128, 128), 128)
+                        there = pl.ds(pl.multiple_of(j * chunk_w + q * 128, 128), 128)
+                        total = part[slots(b), here].astype(F32)
+                        for p in range(1, tps):
+                            total = total + part_in[p - 1, slots(b), there].astype(F32)
+                        target[i, 0:CAP, there] = (scale[slots(b), :] * total).astype(BF16)
+
+                loop(0, half, one)
+
+            fill(outbox, other(bits - 1))
             reduce(bits - 1, j).start()
-            first = kept(bits - 1)
-            loop(first, first + half, one)
+            fill(pair, kept(bits - 1))
 
     def down_step(d):
         e = ahead(d)
@@ -400,18 +485,23 @@
         def _():
             partial(e).start()
 
-    def owned(i):
-        e = ahead(tps * i + lax.bitwise_xor(tp, lax.rem(group, tps)))
-        return lax.div(e, tps)
+    def owned(i, swap=False):
+        d = tps * i + lax.bitwise_xor(tp, lax.rem(group, tps))
+        return lax.div(ahead(turn(d) if swap else d), tps)
 
     def reduce_step(k, i):
-        j = owned(i)
+        j = owned(i, k < bits - 1)
         reduce(k, j).wait_recv()
+        base = kept(k) - kept(bits - 1)
 
         def one(b):
-            here = rows(kept(k) + b)
-            come = pl.ds(pl.multiple_of(((1 << k) - 1 + b) * tok_rows, 16), tok_rows)
-            total = share[here, features(j)].astype(F32) + arrived[come, features(j)].astype(F32)
+            here = rows(base + b)
+            if k == bits - 1:
+                total = jnp.dot(unpack[b], pair[b, :, features(j)], preferred_element_type=F32)
+            else:
+                come = pl.ds(pl.multiple_of(((1 << k) - 1 + b) * tok_rows, 16), tok_rows)
+                total = share[here, features(j)].astype(F32)
+                total = total + arrived[come, features(j)].astype(F32)
             if k > 0:
                 share[here, features(j)] = total.astype(BF16)
             else:
@@ -424,51 +514,61 @@
             for p in range(1, tps):
                 fan(tp, j, p).start()
 
-    def near_step(d):
-        down_step(d)
-
-        @pl.when(d > 0)
-        def _():
-            add_up(ahead(d - 1))
-
-    loop(0, half, near_step)
-    relays(2, half + 1, early)
-    add_up(ahead(half - 1))
+    def down_steps(lo, hi):
+        def one(d):
+            down_step(d)
+
+            @pl.when(d > lo)
+            def _():
+                add_up(ahead(d - 1))
+
+        with phase("down"):
+            loop(lo, hi, one)
+
+    down_steps(0, half)
+    with phase("relay_early"):
+        relays(2, half, early)
+    with phase("near_add"):
+        add_up(ahead(half - 1))
+    down_steps(half, early)
+    with phase("early_add"):
+        add_up(ahead(early - 1))
     for k in range(bits - 1, 0, -1):
-        loop(0, n_w // 2, lambda i, k=k: reduce_step(k, i))
-
-    def far_step(d):
-        down_step(d)
-
-        @pl.when(d > half)
-        def _():
-            add_up(ahead(d - 1))
-
-        @pl.when(d + early - half < experts)
-        def _():
-            relay_step(2, d + early - half)
-
-    loop(half, experts, far_step)
+        with phase(f"near_reduce{k}"):
+            loop(0, n_w // 2, lambda i, k=k: reduce_step(k, i))
+        with phase("relay_late"):
+            lo = early + (bits - 1 - k) * (experts - early) // (bits - 1)
+            relays(2, lo, early + (bits - k) * (experts - early) // (bits - 1))
+    down_steps(early, experts)
     out_copy(2).start()
-    add_up(ahead(experts - 1))
+    with phase("far_add"):
+        add_up(ahead(experts - 1))
     for k in range(bits - 1, 0, -1):
-        loop(n_w // 2, n_w, lambda i, k=k: reduce_step(k, i))
-    loop(n_w // 2, n_w, lambda i: reduce_step(0, i))
-    loop(0, n_w // 2, lambda i: reduce_step(0, i))
+        with phase(f"far_reduce{k}"):
+            loop(n_w // 2, n_w, lambda i, k=k: reduce_step(k, i))
+    with phase("last_far"):
+        loop(n_w // 2, n_w, lambda i: reduce_step(0, i))
+    with phase("last_near"):
+        loop(0, n_w // 2, lambda i: reduce_step(0, i))
 
     def fan_wait(j):
         for p in range(1, tps):
             fan(mate(tps - p), j, p).wait_recv()
 
-    loop(0, n_w, fan_wait)
+    with phase("fan_wait"):
+        loop(0, n_w, fan_wait)
     last_copy = pltpu.make_async_copy(mixed, mixed_out, tok_sem)
     last_copy.start()
 
+    for o in range(experts):
+        for b in masks:
+            if o == 0 or b < o & -o:
+                gather(o, b).wait_send()
+                share_table(o, b).wait_send()
+        for p in range(1, tps):
+            if o:
+                spread(o, tp, p).wait_send()
     for k in range(bits):
-        gather(k, kept(k)).wait_send()
-        share_table(k, kept(k)).wait_send()
-        for p in range(1, tps):
-            spread(k, tp, p).wait_send()
         loop(0, n_w, lambda j, k=k: reduce(k, j).wait_send())
     for m in range(3):
         loop(1, experts, lambda d, m=m: direct(m, ahead(d), group).wait_send())
@@ -501,7 +601,8 @@
     copies = fs_count // experts
     tok_rows, width = tokens.shape
     block = width // tps
-    n_rows = experts * tok_rows
+    n_rows, n_slots = experts * tok_rows, experts * CAP
+    lanes, half = -(-tok_rows // 128) * 128, experts // 2
     depth = shard * fs_count
     n_w = experts // tps
     bits = experts.bit_length() - 1
@@ -524,25 +625,30 @@
             pltpu.VMEM((3, experts, shard, cols), BF16),
             pltpu.VMEM((3, depth, cols), BF16),
             pltpu.VMEM((n_rows, width), BF16),
-            pltpu.VMEM((experts, experts, -(-tok_rows // 128) * 128), F32),
-            pltpu.VMEM((n_rows, 128), F32),
-            pltpu.VMEM((n_rows, cols), BF16),
-            pltpu.VMEM((n_rows, width), BF16),
-            pltpu.VMEM((tps - 1, n_rows, block), BF16),
-            pltpu.VMEM((n_rows, block), BF16),
-            pltpu.VMEM((n_rows - tok_rows, block), BF16),
+            pltpu.VMEM((experts, experts, lanes), F32),
+            pltpu.VMEM((experts, experts, lanes), F32),
+            pltpu.VMEM((n_slots, width), BF16),
+            pltpu.VMEM((half, tok_rows, 2 * CAP), BF16),
+            pltpu.VMEM((n_slots, 128), F32),
+            pltpu.VMEM((n_slots, cols), BF16),
+            pltpu.VMEM((n_slots, width), BF16),
+            pltpu.VMEM((tps - 1, n_slots, block), BF16),
+            pltpu.VMEM((half, CAP, block), BF16),
+            pltpu.VMEM((half, 2 * CAP, block), BF16),
+            pltpu.VMEM((half * tok_rows, block), BF16),
+            pltpu.VMEM(((half - 1) * tok_rows, block), BF16),
             pltpu.VMEM((tok_rows, width), BF16),
             dma((3, experts)),
             dma((3, experts)),
             dma((3, experts)),
             dma((3, experts, copies)),
             dma((3, experts, copies)),
-            dma((bits,)),
-            dma((bits,)),
-            dma((bits,)),
-            dma((bits,)),
-            dma((bits, tps)),
-            dma((bits, tps)),
+            dma((experts,)),
+            dma((experts,)),
+            dma((experts,)),
+            dma((experts,)),
+            dma((experts, tps)),
+            dma((experts, tps)),
             dma((experts,)),
             dma((tps - 1, n_w)),
             dma((bits, n_w)),

time: 267 us -> 215 us (0.81); the launches traced: 262 us -> 215 us
  Pallas kernels: 249 us -> 202 us
    pallas_call x1, Pallas kernels: 249 us -> 202 us  [body(): pl.pallas_call(functools.partial(layer, experts, copies, tps), out_shape=...]
where the time goes in v2:
time: 215 us
  Pallas kernels  202 us (94%)
  local copies, waits for them, and re-layouts  12.6 us (6%)
    pallas_call x1, Pallas kernels, body(): pl.pallas_call(functools.partial(layer, experts, copies, tps), out_shape=...  202 us
    unnamed x8, local copies, waits for them, and re-layouts  12.6 us

profile of v2, /device:TPU:1, one launch (start us, length us, event | category | flops | bytes accessed | tf_op | source)
XLA Modules:
  0.0 215.0 jit_solution(6395355217999077855)
XLA Ops:
  0.6 201.7 %layer.1 = (bf16[192,2048]{1,0:T(8,128)(2,1)}, bf16[1,2048,1024]{2,1,0:T(8,128)(2,1)}, bf16[1,2048,1024]{2,1,0:T(8,128)(2,1)}, bf16[1,2048,1024]{2,1,0:T(8,128)(2,1)}) custom-call(bf16[192,2048]{1,0:T(8,128)(2,1)} %tokens.1, s32[2,192]{1,0:T(2,128)} %bitcast.3, f32[2,192]{1,0:T(2,128)} %bitcast.4, f32[1,128]{1,0:T(1,128)} %bitcast.5, ...), custom_call_target="tpu_custom_call" | custom-call | tf_op jit(solution)/shard_map/layer/pallas_call | solution.py:616
  202.4 2.1 copy.15
  204.5 0.0 copy-start.1
  204.5 4.8 %copy.16 = bf16[1,2048,1024]{2,1,0:T(8,128)(2,1)} copy(bf16[1,2048,1024]{2,1,0:T(8,128)(2,1)} %get-tuple-element.9) | data formatting | bytes 8388608
  209.3 0.0 copy-done.1
  209.3 0.0 copy-start
  209.3 2.1 copy.17
  211.4 1.6 copy-done
  213.0 2.0 copy.18
Async XLA Ops:
  204.5 4.8 %copy-start.1 = (bf16[1,2048,1024]{2,1,0:T(8,128)(2,1)S(1)}, bf16[1,2048,1024]{2,1,0:T(8,128)(2,1)}, u32[]{:S(2)}) copy-start(bf16[1,2048,1024]{2,1,0:T(8,128)(2,1)} %get-tuple-element.10) | copy-start | bytes 12582916
  209.3 3.7 %copy-start = (bf16[1,2048,1024]{2,1,0:T(8,128)(2,1)S(1)}, bf16[1,2048,1024]{2,1,0:T(8,128)(2,1)}, u32[]{:S(2)}) copy-start(bf16[1,2048,1024]{2,1,0:T(8,128)(2,1)} %get-tuple-element.11) | copy-start | bytes 12582916

commit v3 on v2

--- a/solution.py
+++ b/solution.py
@@ -9,6 +9,9 @@
 from jax.sharding import PartitionSpec as P
 
 CAP = 96
+STORES = 4
+PARTS = 1
+KERNEL_VMEM = 46 * 1024 * 1024
 MESH = pl.DeviceIdType.MESH
 BF16 = jnp.bfloat16
 F32 = jnp.float32
@@ -25,15 +28,14 @@
     gate_in,
     up_in,
     down_in,
-    mixed_out,
-    gate_out,
-    up_out,
-    down_out,
+    mixed,
+    gate_full,
+    up_full,
+    down_full,
     tok,
     gain_col,
     stage,
     send,
-    full,
     rows_in,
     table,
     rank,
@@ -47,7 +49,6 @@
     pair,
     share,
     arrived,
-    mixed,
     load_sem,
     w_send,
     w_recv,
@@ -65,7 +66,6 @@
     g_recv,
     f_send,
     f_recv,
-    out_sem,
     tok_sem,
 ):
     shard, cols = stage.shape[2], stage.shape[3]
@@ -81,7 +81,7 @@
     group = lax.div(me, copies)
     lane = lax.rem(me, copies)
     weights = (gate_in, up_in, down_in)
-    outs = (gate_out, up_out, down_out)
+    full = (gate_full, up_full, down_full)
 
     def mirror(o):
         return int(f"{o:0{bits}b}"[::-1], 2)
@@ -123,8 +123,19 @@
     def own_cols(q):
         return pl.ds(pl.multiple_of(q * block, 128), block)
 
-    def features(e):
-        return pl.ds(pl.multiple_of(e * chunk_w, 128), chunk_w)
+    n_sub = min(max(chunk_w // 128, 1), copies)
+    sub_w, lanes_in = chunk_w // n_sub, copies // n_sub
+
+    def piece(t):
+        return lax.rem(lax.div(lane, lanes_in) + t, n_sub)
+
+    def features(e, v=None):
+        if v is None:
+            return pl.ds(pl.multiple_of(e * chunk_w, 128), chunk_w)
+        return pl.ds(pl.multiple_of(e * chunk_w + v * sub_w, 128), sub_w)
+
+    def mark(v):
+        return 0 if v is None else v
 
     def shard_rows(g, c):
         return pl.ds(pl.multiple_of((g * copies + c) * shard, 32), shard)
@@ -149,22 +160,26 @@
     def load(m, h):
         return pltpu.make_async_copy(weights[m].at[h], stage.at[m, h], load_sem.at[m, h])
 
-    def direct(m, h, s):
+    def half_rows(g, c, r):
+        at = (g * copies + c) * shard + r * (shard // PARTS)
+        return pl.ds(pl.multiple_of(at, 16), shard // PARTS)
+
+    def direct(m, h, s, r):
         return remote(
-            send.at[m, h],
-            full.at[m, shard_rows(s, lane)],
-            w_send.at[m, h],
-            w_recv.at[m, s],
+            send.at[m, h, pl.ds(r * (shard // PARTS), shard // PARTS)],
+            full[m].at[0, half_rows(s, lane, r)],
+            w_send.at[m, h, r],
+            w_recv.at[m, s, r],
             h * copies + lane,
             tp,
         )
 
-    def relay(m, s, c, to):
+    def relay(m, s, c, to, r):
         return remote(
-            full.at[m, shard_rows(s, c)],
-            full.at[m, shard_rows(s, c)],
-            r_send.at[m, s, to],
-            r_recv.at[m, s, c],
+            full[m].at[0, half_rows(s, c, r)],
+            full[m].at[0, half_rows(s, c, r)],
+            r_send.at[m, s, to, r],
+            r_recv.at[m, s, c, r],
             group * copies + to,
             tp,
         )
@@ -190,37 +205,39 @@
         span = rows_in.at[rows(at_offset(o)), own_cols(q)]
         return remote(span, span, tx_send.at[o, p], tx_recv.at[o, p], me, mate(p))
 
-    def partial(e):
+    def partial(e, v=None):
         owner, j = lax.rem(e, tps), lax.div(e, tps)
         p = lax.rem(owner - tp + tps, tps)
         return remote(
-            part.at[:, features(e)],
-            part_in.at[p - 1, :, features(j)],
-            p_send.at[e],
-            p_recv.at[p - 1, j],
+            part.at[:, features(e, v)],
+            part_in.at[p - 1, :, features(j, v)],
+            p_send.at[e, mark(v)],
+            p_recv.at[p - 1, j, mark(v)],
             me,
             owner,
         )
 
-    def partial_in(p, j):
-        span = part_in.at[p - 1, :, features(j)]
-        return remote(span, span, p_send.at[0], p_recv.at[p - 1, j], me, mate(p))
+    def partial_in(p, j, v=None):
+        span = part_in.at[p - 1, :, features(j, v)]
+        return remote(span, span, p_send.at[0, 0], p_recv.at[p - 1, j, mark(v)], me, mate(p))
 
     def landing(k):
         return pl.ds(((1 << k) - 1) * tok_rows, tok_rows << k)
 
-    def reduce(k, j):
+    def reduce(k, j, v=None):
         if k == bits - 1:
-            src = outbox.at[:, :, features(j)]
-            dst = pair.at[:, pl.ds(CAP, CAP), features(j)]
+            src = outbox.at[:, :, features(j, v)]
+            dst = pair.at[:, pl.ds(CAP, CAP), features(j, v)]
         else:
-            src = share.at[rows(other(k) - kept(bits - 1), k), features(j)]
-            dst = arrived.at[landing(k), features(j)]
-        return remote(src, dst, g_send.at[k, j], g_recv.at[k, j], hop(k), tp)
-
-    def fan(q, j, p):
-        span = mixed.at[:, features(j * tps + q)]
-        return remote(span, span, f_send.at[j, p], f_recv.at[j, p], me, mate(p))
+            src = share.at[rows(other(k) - kept(bits - 1), k), features(j, v)]
+            dst = arrived.at[landing(k), features(j, v)]
+        return remote(src, dst, g_send.at[k, j, mark(v)], g_recv.at[k, j, mark(v)], hop(k), tp)
+
+    def fan(q, j, p, v=None):
+        span = mixed.at[:, features(j * tps + q, v)]
+        return remote(
+            span, span, f_send.at[j, p, mark(v)], f_recv.at[j, p, mark(v)], me, mate(p)
+        )
 
     tok_copy = pltpu.make_async_copy(tokens, tok, tok_sem)
     tok_copy.start()
@@ -274,7 +291,7 @@
             value = gain_col[...] * value
         return value.astype(BF16)
 
-    full[0, shard_rows(group, lane)] = rounded(0, group)
+    full[0][0, shard_rows(group, lane)] = rounded(0, group)
 
     with phase("barrier"):
         pl.semaphore_wait(barrier, experts + copies + tps - 3)
@@ -296,21 +313,28 @@
         loop(lo, hi, one)
 
     def start(m, lo, hi):
-        loop(lo, hi, lambda d: direct(m, ahead(d), group).start())
+        def one(d):
+            for r in range(PARTS):
+                direct(m, ahead(d), group, r).start()
+
+        loop(lo, hi, one)
 
     def relay_own(m):
         for c in range(1, copies):
-            relay(m, group, lane, twin(c)).start()
+            for r in range(PARTS):
+                relay(m, group, lane, twin(c), r).start()
 
     def relay_step(m, d):
-        s = ahead(turn(d) if m < 2 else d)
-        direct(m, s, s).wait_recv()
-        for c in range(1, copies):
-            relay(m, s, lane, twin(c)).start()
+        s = ahead(turn(d))
+        for r in range(PARTS):
+            direct(m, s, s, r).wait_recv()
+            for c in range(1, copies):
+                relay(m, s, lane, twin(c), r).start()
 
     def relay_wait(m, s):
         for c in range(1, copies):
-            relay(m, s, twin(c), lane).wait_recv()
+            for r in range(PARTS):
+                relay(m, s, twin(c), lane, r).wait_recv()
 
     def gathered(o):
         gather_in(o)
@@ -320,9 +344,6 @@
 
     def relays(m, lo, hi):
         loop(lo, hi, lambda d: relay_step(m, d))
-
-    def out_copy(m):
-        return pltpu.make_async_copy(full.at[m], outs[m].at[0], out_sem.at[m])
 
     early = half + max(half // 2, 1)
     with phase("first"):
@@ -331,7 +352,7 @@
         start(0, 2, early)
         convert(0, 1, 2)
         for m in range(1, 3):
-            full[m, shard_rows(group, lane)] = rounded(m, group)
+            full[m][0, shard_rows(group, lane)] = rounded(m, group)
             start(m - 1, 1, 2)
             convert(m, 1, 2)
             relay_own(m)
@@ -415,7 +436,7 @@
                         relay_step(m + 1, d)
 
             where = pl.ds(pl.multiple_of(c * chunk_f, 128), chunk_f)
-            out = jnp.dot(packed[...], full[m, :, where], preferred_element_type=F32)
+            out = jnp.dot(packed[...], full[m][0, :, where], preferred_element_type=F32)
             if m == 0:
                 out = out / (1.0 + jnp.exp(-out))
             else:
@@ -427,19 +448,43 @@
 
     with phase("gate_wait"):
         loop(0, experts, lambda s: relay_wait(0, s))
-        out_copy(0).start()
     project(0, [(i, 2 + i) for i in range(half)])
 
     @pl.when(jnp.logical_not(at_end))
     def _():
         start(2, half, experts)
 
+    def directs_sent(m, lo, hi):
+        def one(d):
+            for r in range(PARTS):
+                direct(m, ahead(d), group, r).wait_send()
+
+        loop(lo, hi, one)
+
+    def relays_sent(m, lo, hi):
+        def one(d):
+            for c in range(1, copies):
+                for r in range(PARTS):
+                    relay(m, ahead(turn(d)), lane, twin(c), r).wait_send()
+
+        loop(lo, hi, one)
+
+    with phase("sent_0"):
+        for o in range(experts):
+            for b in masks:
+                if o == 0 or b < o & -o:
+                    gather(o, b).wait_send()
+                    share_table(o, b).wait_send()
+            for p in range(1, tps):
+                if o:
+                    spread(o, tp, p).wait_send()
+        directs_sent(0, 1, experts)
+        relays_sent(0, 0, experts)
     with phase("up_rest"):
         relays(1, 2 + half, experts)
 
     with phase("up_wait"):
         loop(0, experts, lambda s: relay_wait(1, s))
-        out_copy(1).start()
 
     @pl.when(at_end)
     def _():
@@ -447,152 +492,210 @@
 
     project(1, [(2 * i, 2 + i) for i in range(half - 2)])
 
-    def add_up(e):
+    def add_up(d, v=None):
+        e = ahead(turn(d))
+
         @pl.when(lax.rem(e, tps) == tp)
         def _():
             j = lax.div(e, tps)
             for p in range(1, tps):
-                partial_in(p, j).wait_recv()
+                partial_in(p, j, v).wait_recv()
+            wide = chunk_w if v is None else sub_w
+            step = min(wide, 128)
+            skip = 0 if v is None else v * sub_w
 
             def fill(target, first):
                 def one(i):
                     b = first + i
-                    for q in range(chunk_w // 128):
-                        here = pl.ds(pl.multiple_of(e * chunk_w + q * 128, 128), 128)
-                        there = pl.ds(pl.multiple_of(j * chunk_w + q * 128, 128), 128)
+                    for q in range(0, wide, step):
+                        here = pl.ds(pl.multiple_of(e * chunk_w + skip + q, step), step)
+                        there = pl.ds(pl.multiple_of(j * chunk_w + skip + q, step), step)
                         total = part[slots(b), here].astype(F32)
                         for p in range(1, tps):
                             total = total + part_in[p - 1, slots(b), there].astype(F32)
-                        target[i, 0:CAP, there] = (scale[slots(b), :] * total).astype(BF16)
+                        target[i, 0:CAP, there] = (scale[slots(b), 0:step] * total).astype(BF16)
 
                 loop(0, half, one)
 
             fill(outbox, other(bits - 1))
-            reduce(bits - 1, j).start()
+            reduce(bits - 1, j, v).start()
             fill(pair, kept(bits - 1))
 
-    def down_step(d):
-        e = ahead(d)
-        relay_wait(2, e)
-        part[:, features(e)] = lax.dot_general(
+    def down_step(d, v=None):
+        e = ahead(turn(d))
+        if v is None:
+            relay_wait(2, e)
+        else:
+            for c in range(lanes_in):
+                source = v * lanes_in + c
+
+                @pl.when(source != lane)
+                def _():
+                    for r in range(PARTS):
+                        relay(2, e, source, lane, r).wait_recv()
+
+        part[:, features(e, v)] = lax.dot_general(
             hidden[...],
-            full[2, features(e), :],
+            full[2][0, features(e, v), :],
             (((1,), (1,)), ((), ())),
             preferred_element_type=F32,
         ).astype(BF16)
 
         @pl.when(lax.rem(e, tps) != tp)
         def _():
-            partial(e).start()
-
-    def owned(i, swap=False):
-        d = tps * i + lax.bitwise_xor(tp, lax.rem(group, tps))
-        return lax.div(ahead(turn(d) if swap else d), tps)
-
-    def reduce_step(k, i):
-        j = owned(i, k < bits - 1)
-        reduce(k, j).wait_recv()
+            partial(e, v).start()
+
+    def owned(i, q):
+        d = tps * i + lax.bitwise_xor(q, lax.rem(group, tps))
+        return lax.div(ahead(turn(d)), tps)
+
+    def reduce_step(k, i, v=None, onward=True):
+        j = owned(i, tp)
+        reduce(k, j, v).wait_recv()
         base = kept(k) - kept(bits - 1)
 
         def one(b):
             here = rows(base + b)
             if k == bits - 1:
-                total = jnp.dot(unpack[b], pair[b, :, features(j)], preferred_element_type=F32)
+                total = jnp.dot(unpack[b], pair[b, :, features(j, v)], preferred_element_type=F32)
             else:
                 come = pl.ds(pl.multiple_of(((1 << k) - 1 + b) * tok_rows, 16), tok_rows)
-                total = share[here, features(j)].astype(F32)
-                total = total + arrived[come, features(j)].astype(F32)
+                total = share[here, features(j, v)].astype(F32)
+                total = total + arrived[come, features(j, v)].astype(F32)
             if k > 0:
-                share[here, features(j)] = total.astype(BF16)
+                share[here, features(j, v)] = total.astype(BF16)
             else:
-                mixed[:, features(j * tps + tp)] = total.astype(BF16)
+                mixed[:, features(j * tps + tp, v)] = total.astype(BF16)
 
         loop(0, 1 << k, one)
-        if k > 0:
-            reduce(k - 1, j).start()
-        else:
+        if k > 0 and onward:
+            reduce(k - 1, j, v).start()
+        if k == 0:
             for p in range(1, tps):
-                fan(tp, j, p).start()
-
-    def down_steps(lo, hi):
-        def one(d):
-            down_step(d)
-
-            @pl.when(d > lo)
+                fan(tp, j, p, v).start()
+
+    def add_ups(lo, hi, v=None):
+        with phase("add"):
+            loop(lo, hi, lambda d: add_up(d, v))
+
+    def down_steps(lo, hi, v=None):
+        with phase("down"):
+            loop(lo, hi, lambda d: down_step(d, v))
+
+    def reduce_steps(k, lo, hi, v=None, onward=True):
+        with phase(f"reduce{k}"):
+            loop(lo, hi, lambda i: reduce_step(k, i, v, onward))
+
+    def relay_early():
+        with phase("relay_early"):
+            relays(2, half, early)
+
+    near_w = n_w // 2
+    early_w = near_w + near_w // 2
+    later = early + (experts - early) // 2
+    pieces = [piece(t) for t in range(n_sub)]
+    near_pieces = [None] if near_w else pieces
+
+    for v in near_pieces:
+        def near_step(d, v=v):
+            down_step(d, v)
+
+            @pl.when(d > 0)
             def _():
-                add_up(ahead(d - 1))
-
-        with phase("down"):
-            loop(lo, hi, one)
-
-    down_steps(0, half)
-    with phase("relay_early"):
-        relays(2, half, early)
-    with phase("near_add"):
-        add_up(ahead(half - 1))
-    down_steps(half, early)
-    with phase("early_add"):
-        add_up(ahead(early - 1))
+                add_up(d - 1, v)
+
+        with phase("near"):
+            loop(0, half, near_step)
+        add_ups(half - 1, half, v)
+    pl.when(jnp.logical_not(at_end))(relay_early)
+    with phase("sent_1"):
+        directs_sent(1, 1, experts)
+        relays_sent(1, 0, experts)
+        directs_sent(2, 1, half)
+    reduce_steps(bits - 1, 0, near_w)
+    pl.when(at_end)(relay_early)
+    for v in pieces:
+        down_steps(half, early, v)
+    for v in pieces:
+        add_ups(half, early, v)
+    with phase("relay_6"):
+        relays(2, early, later)
+
+    def relay_last():
+        with phase("relay_7"):
+            relays(2, later, experts)
+
+    pl.when(at_end)(relay_last)
+    for k in range(bits - 2, 0, -1):
+        reduce_steps(k, 0, near_w, onward=k > 1)
+    for v in pieces:
+        reduce_steps(bits - 1, near_w, early_w, v)
+    down_steps(early, later, pieces[0])
+    pl.when(jnp.logical_not(at_end))(relay_last)
+    down_steps(later, experts, pieces[0])
+    loop(0, near_w, lambda i: reduce(0, owned(i, tp)).start())
+    add_ups(early, experts, pieces[0])
+    for k in range(bits - 2, 0, -1):
+        for v in pieces:
+            reduce_steps(k, near_w, early_w, v)
+    for v in pieces[1:]:
+        down_steps(early, experts, v)
+    for v in pieces[1:]:
+        add_ups(early, experts, v)
     for k in range(bits - 1, 0, -1):
-        with phase(f"near_reduce{k}"):
-            loop(0, n_w // 2, lambda i, k=k: reduce_step(k, i))
-        with phase("relay_late"):
-            lo = early + (bits - 1 - k) * (experts - early) // (bits - 1)
-            relays(2, lo, early + (bits - k) * (experts - early) // (bits - 1))
-    down_steps(early, experts)
-    out_copy(2).start()
-    with phase("far_add"):
-        add_up(ahead(experts - 1))
-    for k in range(bits - 1, 0, -1):
-        with phase(f"far_reduce{k}"):
-            loop(n_w // 2, n_w, lambda i, k=k: reduce_step(k, i))
+        for v in pieces:
+            reduce_steps(k, early_w, n_w, v)
+    def part_sent(d, v=None):
+        @pl.when(lax.rem(ahead(d), tps) != tp)
+        def _():
+            partial(ahead(d), v).wait_send()
+
+    with phase("sent_2"):
+        directs_sent(2, half, experts)
+        relays_sent(2, 0, experts)
+        for v in near_pieces:
+            loop(0, half, lambda d, v=v: part_sent(d, v))
+        for v in pieces:
+            loop(half, experts, lambda d, v=v: part_sent(d, v))
+        for k in range(1, bits):
+            loop(0, near_w, lambda i, k=k: reduce(k, owned(i, tp)).wait_send())
+            for v in pieces:
+                loop(near_w, n_w, lambda i, k=k, v=v: reduce(k, owned(i, tp), v).wait_send())
     with phase("last_far"):
-        loop(n_w // 2, n_w, lambda i: reduce_step(0, i))
+        for v in near_pieces:
+            loop(near_w, n_w, lambda i, v=v: reduce_step(0, i, v))
     with phase("last_near"):
-        loop(0, n_w // 2, lambda i: reduce_step(0, i))
-
-    def fan_wait(j):
+        for v in pieces:
+            loop(0, near_w, lambda i, v=v: reduce_step(0, i, v))
+
+    with phase("fan_wait"):
         for p in range(1, tps):
-            fan(mate(tps - p), j, p).wait_recv()
-
-    with phase("fan_wait"):
-        loop(0, n_w, fan_wait)
-    last_copy = pltpu.make_async_copy(mixed, mixed_out, tok_sem)
-    last_copy.start()
-
-    for o in range(experts):
-        for b in masks:
-            if o == 0 or b < o & -o:
-                gather(o, b).wait_send()
-                share_table(o, b).wait_send()
-        for p in range(1, tps):
-            if o:
-                spread(o, tp, p).wait_send()
-    for k in range(bits):
-        loop(0, n_w, lambda j, k=k: reduce(k, j).wait_send())
-    for m in range(3):
-        loop(1, experts, lambda d, m=m: direct(m, ahead(d), group).wait_send())
-
-        def relays_sent(s, m=m):
-            for c in range(1, copies):
-                relay(m, s, lane, twin(c)).wait_send()
-
-        loop(0, experts, relays_sent)
-        out_copy(m).wait()
-
-    def part_sent(e):
-        @pl.when(lax.rem(e, tps) != tp)
-        def _():
-            partial(e).wait_send()
-
-    loop(0, experts, part_sent)
-
-    def fans_sent(j):
-        for p in range(1, tps):
-            fan(tp, j, p).wait_send()
-
-    loop(0, n_w, fans_sent)
-    last_copy.wait()
+            q = mate(tps - p)
+            for v in near_pieces:
+                loop(near_w, n_w, lambda i, p=p, q=q, v=v: fan(q, owned(i, q), p, v).wait_recv())
+            for v in pieces:
+                loop(0, near_w, lambda i, p=p, q=q, v=v: fan(q, owned(i, q), p, v).wait_recv())
+    loop(0, near_w, lambda i: reduce(0, owned(i, tp)).wait_send())
+    for v in pieces:
+        loop(near_w, n_w, lambda i, v=v: reduce(0, owned(i, tp), v).wait_send())
+    for p in range(1, tps):
+        for v in near_pieces:
+            loop(near_w, n_w, lambda i, p=p, v=v: fan(tp, owned(i, tp), p, v).wait_send())
+        for v in pieces:
+            loop(0, near_w, lambda i, p=p, v=v: fan(tp, owned(i, tp), p, v).wait_send())
+
+
+def store(*refs):
+    copies = [pltpu.make_async_copy(refs[0], refs[4], refs[-1].at[0, 0])]
+    for i in range(1, 4):
+        size = refs[i].shape[1] // STORES
+        for k in range(STORES):
+            at = (slice(None), pl.ds(k * size, size))
+            copies.append(pltpu.make_async_copy(refs[i].at[at], refs[4 + i].at[at], refs[-1].at[i, k]))
+    for copy in copies:
+        copy.start()
+    for copy in copies:
+        copy.wait()
 
 
 def body(tokens, route_ids, route_logits, norm_gain, gate_weight, up_weight, down_weight):
@@ -603,6 +706,8 @@
     block = width // tps
     n_rows, n_slots = experts * tok_rows, experts * CAP
     lanes, half = -(-tok_rows // 128) * 128, experts // 2
+    n_sub = min(max(width // experts // 128, 1), copies)
+    assert copies % n_sub == 0
     depth = shard * fs_count
     n_w = experts // tps
     bits = experts.bit_length() - 1
@@ -612,18 +717,17 @@
     dma = pltpu.SemaphoreType.DMA
     anywhere = pl.BlockSpec(memory_space=pl.ANY)
     inside = pl.BlockSpec(memory_space=pltpu.VMEM)
-    copy_shape = jax.ShapeDtypeStruct((1, depth, cols), BF16)
-    return pl.pallas_call(
+    shapes = ((tok_rows, width),) + ((1, depth, cols),) * 3
+    results = pl.pallas_call(
         functools.partial(layer, experts, copies, tps),
-        out_shape=(jax.ShapeDtypeStruct((tok_rows, width), BF16),) + (copy_shape,) * 3,
+        out_shape=tuple(pltpu.VMEM(shape, BF16) for shape in shapes),
         in_specs=[anywhere] + [inside] * 3 + [anywhere] * 3,
-        out_specs=(anywhere,) * 4,
+        out_specs=(inside,) * 4,
         scratch_shapes=[
             pltpu.VMEM((tok_rows, width), BF16),
             pltpu.VMEM((shard, 1), F32),
             pltpu.VMEM((3, experts, shard, cols), F32),
             pltpu.VMEM((3, experts, shard, cols), BF16),
-            pltpu.VMEM((3, depth, cols), BF16),
             pltpu.VMEM((n_rows, width), BF16),
             pltpu.VMEM((experts, experts, lanes), F32),
             pltpu.VMEM((experts, experts, lanes), F32),
@@ -637,29 +741,27 @@
             pltpu.VMEM((half, 2 * CAP, block), BF16),
             pltpu.VMEM((half * tok_rows, block), BF16),
             pltpu.VMEM(((half - 1) * tok_rows, block), BF16),
-            pltpu.VMEM((tok_rows, width), BF16),
             dma((3, experts)),
-            dma((3, experts)),
-            dma((3, experts)),
-            dma((3, experts, copies)),
-            dma((3, experts, copies)),
+            dma((3, experts, PARTS)),
+            dma((3, experts, PARTS)),
+            dma((3, experts, copies, PARTS)),
+            dma((3, experts, copies, PARTS)),
             dma((experts,)),
             dma((experts,)),
             dma((experts,)),
             dma((experts,)),
             dma((experts, tps)),
             dma((experts, tps)),
-            dma((experts,)),
-            dma((tps - 1, n_w)),
-            dma((bits, n_w)),
-            dma((bits, n_w)),
-            dma((n_w, tps)),
-            dma((n_w, tps)),
-            dma((3,)),
+            dma((experts, n_sub)),
+            dma((tps - 1, n_w, n_sub)),
+            dma((bits, n_w, n_sub)),
+            dma((bits, n_w, n_sub)),
+            dma((n_w, tps, n_sub)),
+            dma((n_w, tps, n_sub)),
             dma,
         ],
         compiler_params=pltpu.CompilerParams(
-            collective_id=0, has_side_effects=True, vmem_limit_bytes=64 * 1024 * 1024 - 65536
+            collective_id=0, has_side_effects=True, vmem_limit_bytes=KERNEL_VMEM
         ),
         name="layer",
     )(
@@ -671,6 +773,15 @@
         up_weight,
         down_weight,
     )
+    return pl.pallas_call(
+        store,
+        out_shape=tuple(jax.ShapeDtypeStruct(shape, BF16) for shape in shapes),
+        in_specs=[inside] * 4,
+        out_specs=(anywhere,) * 4,
+        scratch_shapes=[dma((4, STORES))],
+        compiler_params=pltpu.CompilerParams(vmem_limit_bytes=1024 * 1024),
+        name="store",
+    )(*results)
 
 
 def solution(mesh):

time: 215 us -> 197 us (0.916); the launches traced: 215 us -> 194 us
  local copies, waits for them, and re-layouts: 12.6 us -> 0 us
  Pallas kernels: 202 us -> 193 us
    pallas_call x1, Pallas kernels: 202 us -> 189 us  [body(): pl.pallas_call(functools.partial(layer, experts, copies, tps), out_shape=...]
    unnamed x8 -> x0, local copies, waits for them, and re-layouts: 12.6 us -> none
    pallas_call x0 -> x1, Pallas kernels: none -> 4.96 us  [body(): pl.pallas_call(store, out_shape=tuple((jax.ShapeDtypeStruct(shape, BF16)...]
where the time goes in v3:
time: 197 us; the launch traced here: 194 us
  Pallas kernels  193 us (98%)
    pallas_call x1, Pallas kernels, body(): pl.pallas_call(functools.partial(layer, experts, copies, tps), out_shape=...  189 us
    pallas_call x1, Pallas kernels, body(): pl.pallas_call(store, out_shape=tuple((jax.ShapeDtypeStruct(shape, BF16)...  4.96 us

profile of v3, /device:TPU:1, one launch (start us, length us, event | category | flops | bytes accessed | tf_op | source)
XLA Modules:
  0.0 194.1 jit_solution(5879453651348569309)
XLA Ops:
  0.6 188.5 %layer.1 = (bf16[192,2048]{1,0:T(8,128)(2,1)S(1)}, bf16[1,2048,1024]{2,1,0:T(8,128)(2,1)S(1)}, bf16[1,2048,1024]{2,1,0:T(8,128)(2,1)S(1)}, bf16[1,2048,1024]{2,1,0:T(8,128)(2,1)S(1)}) custom-call(bf16[192,2048]{1,0:T(8,128)(2,1)} %tokens.1, s32[2,192]{1,0:T(2,128)} %bitcast.3, f32[2,192]{1,0:T(2,128)} %bitcast.4, f32[1,128]{1,0:T(1,128)} %bitcast.5, ...), custom_call_target="tpu_custom_call" | custom-call | tf_op jit(solution)/shard_map/layer/pallas_call | solution.py:721
  189.2 5.0 %store.1 = (bf16[192,2048]{1,0:T(8,128)(2,1)}, bf16[1,2048,1024]{2,1,0:T(8,128)(2,1)}, bf16[1,2048,1024]{2,1,0:T(8,128)(2,1)}, bf16[1,2048,1024]{2,1,0:T(8,128)(2,1)}) custom-call(bf16[192,2048]{1,0:T(8,128)(2,1)S(1)} %get-tuple-element.8.refs_0_, bf16[1,2048,1024]{2,1,0:T(8,128)(2,1)S(1)} %get-tuple-element.9.refs_1_, ...), custom_call_target="tpu_custom_call" | custom-call | tf_op jit(solution)/shard_map/store/pallas_call | solution.py:776

commit v4 on v3

--- a/solution.py
+++ b/solution.py
@@ -452,7 +452,7 @@
 
     @pl.when(jnp.logical_not(at_end))
     def _():
-        start(2, half, experts)
+        start(2, half, early)
 
     def directs_sent(m, lo, hi):
         def one(d):
@@ -486,11 +486,12 @@
     with phase("up_wait"):
         loop(0, experts, lambda s: relay_wait(1, s))
 
+    project(1, [(2 * i, 2 + i) for i in range(half - 2)])
+
     @pl.when(at_end)
     def _():
         start(2, half, experts)
 
-    project(1, [(2 * i, 2 + i) for i in range(half - 2)])
 
     def add_up(d, v=None):
         e = ahead(turn(d))
@@ -608,6 +609,10 @@
             loop(0, half, near_step)
         add_ups(half - 1, half, v)
     pl.when(jnp.logical_not(at_end))(relay_early)
+    @pl.when(jnp.logical_not(at_end))
+    def _():
+        start(2, early, experts)
+
     with phase("sent_1"):
         directs_sent(1, 1, experts)
         relays_sent(1, 0, experts)
@@ -631,9 +636,9 @@
     for v in pieces:
         reduce_steps(bits - 1, near_w, early_w, v)
     down_steps(early, later, pieces[0])
+    loop(0, near_w, lambda i: reduce(0, owned(i, tp)).start())
     pl.when(jnp.logical_not(at_end))(relay_last)
     down_steps(later, experts, pieces[0])
-    loop(0, near_w, lambda i: reduce(0, owned(i, tp)).start())
     add_ups(early, experts, pieces[0])
     for k in range(bits - 2, 0, -1):
         for v in pieces:

time: 197 us -> 194 us (0.985); the launches traced: 194 us -> 194 us
  no operation moved by 1% of the time
where the time goes in v4:
time: 194 us
  Pallas kernels  194 us (100%)
    pallas_call x1, Pallas kernels, body(): pl.pallas_call(functools.partial(layer, experts, copies, tps), out_shape=...  189 us
    pallas_call x1, Pallas kernels, body(): pl.pallas_call(store, out_shape=tuple((jax.ShapeDtypeStruct(shape, BF16)...  4.96 us

profile of v4, /device:TPU:1, one launch (start us, length us, event | category | flops | bytes accessed | tf_op | source)
XLA Modules:
  0.0 194.2 jit_solution(14222249327430475389)
XLA Ops:
  0.6 188.6 %layer.1 = (bf16[192,2048]{1,0:T(8,128)(2,1)S(1)}, bf16[1,2048,1024]{2,1,0:T(8,128)(2,1)S(1)}, bf16[1,2048,1024]{2,1,0:T(8,128)(2,1)S(1)}, bf16[1,2048,1024]{2,1,0:T(8,128)(2,1)S(1)}) custom-call(bf16[192,2048]{1,0:T(8,128)(2,1)} %tokens.1, s32[2,192]{1,0:T(2,128)} %bitcast.3, f32[2,192]{1,0:T(2,128)} %bitcast.4, f32[1,128]{1,0:T(1,128)} %bitcast.5, ...), custom_call_target="tpu_custom_call" | custom-call | tf_op jit(solution)/shard_map/layer/pallas_call | solution.py:726
  189.2 5.0 %store.1 = (bf16[192,2048]{1,0:T(8,128)(2,1)}, bf16[1,2048,1024]{2,1,0:T(8,128)(2,1)}, bf16[1,2048,1024]{2,1,0:T(8,128)(2,1)}, bf16[1,2048,1024]{2,1,0:T(8,128)(2,1)}) custom-call(bf16[192,2048]{1,0:T(8,128)(2,1)S(1)} %get-tuple-element.8.refs_0_, bf16[1,2048,1024]{2,1,0:T(8,128)(2,1)S(1)} %get-tuple-element.9.refs_1_, ...), custom_call_target="tpu_custom_call" | custom-call | tf_op jit(solution)/shard_map/store/pallas_call | solution.py:781
